TPU v7x, 1024 devices: a whole 4x8x16 slice. The times are simulated.
1024 devices in a mesh: fs: 32 (over z, core), tp: 32 (over y, x).
Axes of the slice: x: 4, y: 8, z: 16, core: 2. Of those that a mesh axis runs over, the one named last changes fastest.
Arguments:
- tokens: bfloat16 [4096, 2048], P('fs', 'tp'), may hold values from -6 to 6
- first_gain: float32 [2048], P('fs'), may hold values from 0.1 to 1.9
- first_gate: float32 [2048, 5504], P('fs', 'tp'), may hold values from -0.125 to 0.125
- first_up: float32 [2048, 5504], P('fs', 'tp'), may hold values from -0.125 to 0.125
- first_down: float32 [5504, 2048], P('tp', 'fs'), may hold values from -0.15625 to 0.15625
- first_post: float32 [2048], replicated, may hold values from 0.1 to 1.9
- second_gain: float32 [2048], P('fs'), may hold values from 0.1 to 1.9
- second_gate: float32 [2048, 5504], P('fs', 'tp'), may hold values from -0.125 to 0.125
- second_up: float32 [2048, 5504], P('fs', 'tp'), may hold values from -0.125 to 0.125
- second_down: float32 [5504, 2048], P('tp', 'fs'), may hold values from -0.15625 to 0.15625
- second_post: float32 [2048], replicated, may hold values from 0.1 to 1.9
Outputs:
- mixed: bfloat16 [4096, 2048], P('fs', 'tp')
- gate_one: bfloat16 [2048, 5504], P(None, 'tp')
- up_one: bfloat16 [2048, 5504], P(None, 'tp')
- down_one: bfloat16 [5504, 2048], P('tp')
- gate_two: bfloat16 [2048, 5504], P(None, 'tp')
- up_two: bfloat16 [2048, 5504], P(None, 'tp')
- down_two: bfloat16 [5504, 2048], P('tp')
All inputs are finite; a program needn't handle non-finite values.
Results may differ from a plain program's by a relative error of at most 0.015.
Values may be sent and summed in bfloat16 or wider, within the bound.
No kernel may reach another device: no remote copies, remote signals or barrier semaphores. Data moves between devices by JAX's collectives and lax.ppermute only.
A program may use at most 32 MiB of HBM per device.

v0:
```python
import jax
import jax.numpy as jnp
from jax import lax
from jax.sharding import Mesh
from jax.sharding import PartitionSpec as P

D = 2048
TP = ("tp_0", "tp_1")


norm_epsilon = 1e-06


def rows_first(arrays, axis, dims):
    turned = [jnp.moveaxis(a, dim, 0) for a, dim in zip(arrays, dims)]
    both = jnp.concatenate([t.reshape(len(t), -1) for t in turned], axis=1)
    out, at, outs = (lax.all_gather(both, axis, axis=0, tiled=True), 0, [])
    for t, dim in zip(turned, dims):
        piece = out[:, at : at + t[0].size].reshape(-1, *t.shape[1:])
        outs.append(jnp.moveaxis(piece, 0, dim))
        at += t[0].size
    return tuple(outs)


def joined_along(parts, dim):
    parts = jnp.moveaxis(parts, 0, dim)
    shape = parts.shape
    return parts.reshape(*shape[:dim], shape[dim] * shape[dim + 1], *shape[dim + 2 :])


def sent_to_all(x, axis):
    peers = lax.axis_size(axis)
    return lax.all_to_all(jnp.broadcast_to(x[None], (peers, *x.shape)), axis, 0, 0, tiled=True)


def gathered_copies(x, axis, dim):
    return joined_along(sent_to_all(x, axis), dim)


def cut_along(x, dim, peers):
    before, after = (x.shape[:dim], x.shape[dim + 1 :])
    return jnp.moveaxis(x.reshape(*before, peers, -1, *after), dim, 0)


def sent_and_summed(x, axis, dim):
    peers = lax.axis_size(axis)
    parts = lax.all_to_all(cut_along(x, dim, peers), axis, 0, 0, tiled=True)
    return jnp.sum(parts.astype(jnp.float32), axis=0)


def of_everyone(x, axis):
    return sent_to_all(x, axis).sum(axis=0)


def whole_of(x, axes, dim):
    if not axes:
        return x
    nearer = lax.all_gather(x, axes[-1], axis=dim, tiled=True)
    return whole_of(nearer, axes[:-1], dim)


def collect(gain, gate, up, down):
    gate_half = (gain[:, None] * gate).astype(jnp.bfloat16)
    up_half = (gain[:, None] * up).astype(jnp.bfloat16)
    down_half = down.astype(jnp.bfloat16)
    gate_slab, up_slab, down_slab = rows_first((gate_half, up_half, down_half), "fs", (0, 0, 1))
    return (gate_slab, up_slab, down_slab)


def partial_mix(full_rows, slabs):
    rows_float = full_rows.astype(jnp.float32)
    scale = lax.rsqrt(jnp.mean(rows_float * rows_float, axis=1, keepdims=True) + norm_epsilon)
    gate = scale * jnp.dot(full_rows, slabs[0], preferred_element_type=jnp.float32)
    up = scale * jnp.dot(full_rows, slabs[1], preferred_element_type=jnp.float32)
    hidden = (jax.nn.silu(gate) * up).astype(jnp.bfloat16)
    return jnp.dot(hidden, slabs[2], preferred_element_type=jnp.float32)


def on_device(
    tokens,
    first_gain,
    first_gate,
    first_up,
    first_down,
    first_post,
    second_gain,
    second_gate,
    second_up,
    second_down,
    second_post,
):
    columns = tokens.shape[1]
    column_start = lax.axis_index(TP) * columns
    full_rows = gathered_copies(tokens, TP, 1)
    slabs_one = collect(first_gain, first_gate, first_up, first_down)
    slabs_two = collect(second_gain, second_gate, second_up, second_down)

    def finish(own_columns, partial_value, post):
        share = sent_and_summed(partial_value.astype(jnp.bfloat16), TP, 1)
        squares = of_everyone(jnp.sum(share * share, axis=1, keepdims=True), TP)
        scale = lax.rsqrt(squares / D + norm_epsilon)
        gain_part = lax.dynamic_slice_in_dim(post, column_start, columns, 0)
        return (own_columns.astype(jnp.float32) + 0.5 * share * scale * gain_part[None, :]).astype(
            jnp.bfloat16
        )

    middle_columns = finish(tokens, partial_mix(full_rows, slabs_one), first_post)
    middle_full = whole_of(middle_columns, TP, 1)
    mixed = finish(middle_columns, partial_mix(middle_full, slabs_two), second_post)
    return (
        mixed,
        slabs_one[0],
        slabs_one[1],
        slabs_one[2],
        slabs_two[0],
        slabs_two[1],
        slabs_two[2],
    )


def solution(mesh):
    torus = Mesh(mesh.devices.reshape(mesh.shape["fs"], 8, 4), ("fs", "tp_0", "tp_1"))
    in_specs = (
        P("fs", TP),
        P("fs"),
        P("fs", TP),
        P("fs", TP),
        P(TP, "fs"),
        P(),
        P("fs"),
        P("fs", TP),
        P("fs", TP),
        P(TP, "fs"),
        P(),
    )
    out_specs = (
        P("fs", TP),
        P(None, TP),
        P(None, TP),
        P(TP, None),
        P(None, TP),
        P(None, TP),
        P(TP, None),
    )
    return jax.shard_map(
        on_device, mesh=torus, in_specs=in_specs, out_specs=out_specs, check_vma=False
    )
```

profile of v0, /device:TPU:2, one launch (start us, length us, event | category | flops | bytes accessed | tf_op | source)
XLA Modules:
  0.0 232.0 jit_solution(4665715498052010554)
XLA Ops:
  7.2 0.8 convert_bitcast_fusion.1
  8.1 1.0 multiply_convert_fusion.3
  9.8 1.6 broadcast_in_dim.6
  11.4 16.7 %all-to-all-start = ((bf16[32,128,64]{1,2,0:T(8,128)(2,1)}), bf16[32,128,64]{1,2,0:T(8,128)(2,1)S(1)}, u32[]{:S(2)}, u32[]{:S(2)}) async-start(bf16[32,128,64]{1,2,0:T(8,128)(2,1)} %broadcast_in_dim.6), calls=%async_computation | async-start | bytes 1048576 | tf_op jit(solution)/shard_map/all_to_all | solution.py:33
  28.2 1.0 multiply_convert_fusion.1
  29.1 0.8 convert_bitcast_fusion
  30.7 10.1 %all-to-all-done = bf16[32,128,64]{1,2,0:T(8,128)(2,1)S(1)} async-done(((bf16[32,128,64]{1,2,0:T(8,128)(2,1)}), bf16[32,128,64]{1,2,0:T(8,128)(2,1)S(1)}, u32[]{:S(2)}, u32[]{:S(2)}) %all-to-all-start) | async-done | bytes 524320 | tf_op jit(solution)/shard_map/all_to_all | solution.py:33
  41.1 53.6 %all-gather.3.cloned.1.call-done = bf16[2048,516]{1,0:T(8,128)(2,1)} async-done(((bf16[64,516]{1,0:T(8,128)(2,1)}), bf16[2048,516]{1,0:T(8,128)(2,1)}) %all-gather.3.cloned.1.call-update) | async-done | bytes 2113552 | tf_op jit(solution)/shard_map/all_gather | solution.py:17
  94.7 1.7 fusion.3
  96.4 3.2 %convolution_convert_fusion.1 = bf16[128,2048]{1,0:T(8,128)(2,1)S(1)} fusion(bf16[128,2048]{0,1:T(8,128)(2,1)S(1)} %bitcast.33, bf16[2048,516]{1,0:T(8,128)(2,1)} %all-gather.3.cloned.1.call-done, f32[128,172]{0,1:T(8,128)S(1)} %fusion.3, f32[128]{0:T(128)S(1)} %add_rsqrt_fusion.1), kind=kOutput, calls=%fused_computation.1 | convolution fusion | flops 180771328 | bytes 3234304 | tf_op jit(solution)/shard_map/dot_general | solution.py:76
  99.9 26.9 %all_to_all.25 = bf16[32,128,64]{1,2,0:T(8,128)(2,1)S(1)} all-to-all(bf16[32,128,64]{1,2,0:T(8,128)(2,1)S(1)} %bitcast.34), channel_id=1, replica_groups=mesh['fs'=32,'tp_0'=8,'tp_1'=4] {'tp_0','tp_1'}, dimensions={0} | all-to-all | bytes 1048576 | tf_op jit(solution)/shard_map/all_to_all | solution.py:47
  127.5 5.6 %all-to-all-start.2 = ((f32[32,128,1]{1,2,0:T(1,128)}), f32[32,128,1]{1,2,0:T(1,128)S(1)}, u32[]{:S(2)}, u32[]{:S(2)}) async-start(f32[32,128,1]{1,2,0:T(1,128)} %broadcast_in_dim.7), calls=%async_computation.2 | async-start | bytes 32768 | tf_op jit(solution)/shard_map/all_to_all | solution.py:33
  133.1 0.8 dynamic_slice.6
  133.9 7.7 %all-to-all-done.2 = f32[32,128,1]{1,2,0:T(1,128)S(1)} async-done(((f32[32,128,1]{1,2,0:T(1,128)}), f32[32,128,1]{1,2,0:T(1,128)S(1)}, u32[]{:S(2)}, u32[]{:S(2)}) %all-to-all-start.2) | async-done | bytes 16416 | tf_op jit(solution)/shard_map/all_to_all | solution.py:33
  141.7 11.3 %all_gather.13 = bf16[128,256]{0,1:T(8,128)(2,1)S(1)} all-gather(bf16[128,64]{0,1:T(8,128)(2,1)S(1)} %add_convert_fusion.1), channel_id=1, replica_groups=mesh['fs'=32,'tp_0'=8,'tp_1'=4] {'tp_1'}, dimensions={1}, use_global_device_ids=true | all-gather | bytes 81920 | tf_op jit(solution)/shard_map/all_gather | solution.py:58
  153.0 25.3 %all_gather.14 = bf16[128,2048]{0,1:T(8,128)(2,1)S(1)} all-gather(bf16[128,256]{0,1:T(8,128)(2,1)S(1)} %all_gather.13), channel_id=1, replica_groups=mesh['fs'=32,'tp_0'=8,'tp_1'=4] {'tp_0'}, dimensions={1}, use_global_device_ids=true | all-gather | bytes 589824 | tf_op jit(solution)/shard_map/all_gather | solution.py:58
  178.6 1.7 convolution_multiply_fusion.1
  180.3 3.6 %convolution_convert_fusion = bf16[128,2048]{1,0:T(8,128)(2,1)S(1)} fusion(bf16[128,2048]{0,1:T(8,128)(2,1)S(1)} %all_gather.14, bf16[2048,516]{1,0:T(8,128)(2,1)} %all-gather.5.cloned.1.call-done, f32[128,172]{0,1:T(8,128)S(1)} %convolution_multiply_fusion.1, f32[128]{0:T(128)S(1)} %add_rsqrt_fusion), kind=kOutput, calls=%fused_computation | convolution fusion | flops 180771328 | bytes 3234304 | tf_op jit(solution)/shard_map/dot_general | solution.py:76
  184.0 1.0 copy.34
  185.0 6.2 %all-to-all-start.3 = ((bf16[32,128,64]{1,2,0:T(8,128)(2,1)}), bf16[32,128,64]{1,2,0:T(8,128)(2,1)}, u32[]{:S(2)}, u32[]{:S(2)}) async-start(bf16[32,128,64]{1,2,0:T(8,128)(2,1)} %bitcast.10), calls=%async_computation.3 | async-start | bytes 1048576 | tf_op jit(solution)/shard_map/all_to_all | solution.py:47
  191.2 0.8 dynamic_slice.7
  192.0 3.3 %slice_bitcast_fusion.1 = (bf16[172,2048]{0,1:T(8,128)(2,1)S(1)}, bf16[2048,172]{1,0:T(8,128)(2,1)S(1)}, bf16[2048,172]{1,0:T(8,128)(2,1)S(1)}) fusion(bf16[2048,516]{1,0:T(8,128)(2,1)} %all-gather.3.cloned.1.call-done), kind=kLoop, calls=%fused_computation.18 | loop fusion | bytes 4227072 | tf_op jit(solution)/shard_map/transpose | solution.py:20
  195.3 8.7 %all-to-all-done.3 = bf16[32,128,64]{1,2,0:T(8,128)(2,1)} async-done(((bf16[32,128,64]{1,2,0:T(8,128)(2,1)}), bf16[32,128,64]{1,2,0:T(8,128)(2,1)}, u32[]{:S(2)}, u32[]{:S(2)}) %all-to-all-start.3) | async-done | bytes 524320 | tf_op jit(solution)/shard_map/all_to_all | solution.py:47
  204.0 1.1 convert_reduce_fusion
  205.8 5.4 %all-to-all-start.4 = ((f32[32,128,1]{1,2,0:T(1,128)}), f32[32,128,1]{1,2,0:T(1,128)S(1)}, u32[]{:S(2)}, u32[]{:S(2)}) async-start(f32[32,128,1]{1,2,0:T(1,128)} %broadcast_in_dim.8), calls=%async_computation.4 | async-start | bytes 32768 | tf_op jit(solution)/shard_map/all_to_all | solution.py:33
  211.2 4.9 %slice_bitcast_fusion = (bf16[172,2048]{0,1:T(8,128)(2,1)}, bf16[2048,172]{1,0:T(8,128)(2,1)}, bf16[2048,172]{1,0:T(8,128)(2,1)}) fusion(bf16[2048,516]{1,0:T(8,128)(2,1)} %all-gather.5.cloned.1.call-done), kind=kLoop, calls=%fused_computation.16 | loop fusion | bytes 4227072 | tf_op jit(solution)/shard_map/transpose | solution.py:20
  216.2 1.2 copy.35
  217.4 1.2 copy.36
  218.6 1.2 copy.37
  219.8 2.2 copy.38
  221.9 1.2 copy.39
  223.2 1.2 copy.40
  (30 shorter events, 4.7 us)
Async XLA Ops:
  7.2 87.6 %all-gather.3.cloned.1.call-start = ((), (), s32[]{:S(2)}) async-start(), calls=%async_computation.5 | async-start | bytes 2703360 | tf_op jit(solution)/shard_map/all_gather | solution.py:17
  11.4 29.4 %all-to-all-start = ((bf16[32,128,64]{1,2,0:T(8,128)(2,1)}), bf16[32,128,64]{1,2,0:T(8,128)(2,1)S(1)}, u32[]{:S(2)}, u32[]{:S(2)}) async-start(bf16[32,128,64]{1,2,0:T(8,128)(2,1)} %broadcast_in_dim.6), calls=%async_computation | async-start | bytes 1048576 | tf_op jit(solution)/shard_map/all_to_all | solution.py:33
  28.1 150.5 %all-gather.5.cloned.1.call-start = ((), (), s32[]{:S(2)}) async-start(), calls=%async_computation.6 | async-start | bytes 2703360 | tf_op jit(solution)/shard_map/all_gather | solution.py:17
  96.4 45.2 %copy-start.2 = (bf16[128,64]{0,1:T(8,128)(2,1)S(1)}, bf16[128,64]{0,1:T(8,128)(2,1)}, u32[]{:S(2)}) copy-start(bf16[128,64]{0,1:T(8,128)(2,1)} %param.11) | copy-start | bytes 49156
  127.5 14.1 %all-to-all-start.2 = ((f32[32,128,1]{1,2,0:T(1,128)}), f32[32,128,1]{1,2,0:T(1,128)S(1)}, u32[]{:S(2)}, u32[]{:S(2)}) async-start(f32[32,128,1]{1,2,0:T(1,128)} %broadcast_in_dim.7), calls=%async_computation.2 | async-start | bytes 32768 | tf_op jit(solution)/shard_map/all_to_all | solution.py:33
  185.0 19.0 %all-to-all-start.3 = ((bf16[32,128,64]{1,2,0:T(8,128)(2,1)}), bf16[32,128,64]{1,2,0:T(8,128)(2,1)}, u32[]{:S(2)}, u32[]{:S(2)}) async-start(bf16[32,128,64]{1,2,0:T(8,128)(2,1)} %bitcast.10), calls=%async_computation.3 | async-start | bytes 1048576 | tf_op jit(solution)/shard_map/all_to_all | solution.py:47
  205.8 18.6 %all-to-all-start.4 = ((f32[32,128,1]{1,2,0:T(1,128)}), f32[32,128,1]{1,2,0:T(1,128)S(1)}, u32[]{:S(2)}, u32[]{:S(2)}) async-start(f32[32,128,1]{1,2,0:T(1,128)} %broadcast_in_dim.8), calls=%async_computation.4 | async-start | bytes 32768 | tf_op jit(solution)/shard_map/all_to_all | solution.py:33
  217.4 4.6 %copy-start.1 = (bf16[2048,172]{1,0:T(8,128)(2,1)S(1)}, bf16[2048,172]{1,0:T(8,128)(2,1)}, u32[]{:S(2)}) copy-start(bf16[2048,172]{1,0:T(8,128)(2,1)} %get-tuple-element.15) | copy-start | bytes 2113540
  218.6 4.6 %copy-start = (bf16[172,2048]{0,1:T(8,128)(2,1)S(1)}, bf16[172,2048]{0,1:T(8,128)(2,1)}, u32[]{:S(2)}) copy-start(bf16[172,2048]{0,1:T(8,128)(2,1)} %get-tuple-element.14) | copy-start | bytes 2113540
Sparse Core Ops, SparseCore 0:
  11.3 83.4 all-gather.2
  98.0 72.2 all-gather.4
where the time goes:
time: 233 us; the launch traced here: 232 us
  waiting for transfers between devices  80.2 us (34%)
  blocking collectives  63.4 us (27%)
  starting transfers between devices  34 us (15%)
  local copies, waits for them, and re-layouts  22.1 us (9%)
  between operations  14.2 us (6%)
  matrix products  10.3 us (4%)
  other arithmetic  7.83 us (3%)
    all_gather x2, waiting for transfers between devices, rows_first(): out, at, outs = (lax.all_gather(both, axis, axis=0, tiled=True), 0, [])  53.6 us
    all_gather x2, blocking collectives, whole_of(): nearer = lax.all_gather(x, axes[-1], axis=dim, tiled=True)  36.6 us
    all_to_all x3, starting transfers between devices, sent_to_all(): lax.all_to_all(jnp.broadcast_to(x[None], (peers, *x.shape)), axis, 0, 0,...  27.7 us
    all_to_all x1, blocking collectives, sent_and_summed(): parts = lax.all_to_all(cut_along(x, dim, peers), axis, 0, 0, tiled=True)  26.9 us
    all_to_all x3, waiting for transfers between devices, sent_to_all(): lax.all_to_all(jnp.broadcast_to(x[None], (peers, *x.shape)), axis, 0, 0,...  17.8 us
    all_to_all x1, waiting for transfers between devices, sent_and_summed(): parts = lax.all_to_all(cut_along(x, dim, peers), axis, 0, 0, tiled=True)  8.74 us
    unnamed x12, local copies, waits for them, and re-layouts  8.21 us
    transpose x2, local copies, waits for them, and re-layouts, rows_first(): outs.append(jnp.moveaxis(piece, 0, dim))  8.2 us
  transfers between devices with their start and end apart: 6, of which 4 were waited for; matrix products, arithmetic and copies ran while one was open for 12% of the time, Pallas kernels for 0%

commit v1 on v0

v1 whole, which is shorter than its diff:
```python
import jax
import jax.numpy as jnp
from jax import lax
from jax.experimental import pallas as pl
from jax.experimental.pallas import tpu as pltpu
from jax.sharding import Mesh
from jax.sharding import PartitionSpec as P


TP = ("tp_0", "tp_1")
FS = ("pair", "parity", "core")


norm_epsilon = 1e-06


def sent_to_all(x, axis):
    peers = lax.axis_size(axis)
    return lax.all_to_all(jnp.broadcast_to(x[None], (peers, *x.shape)), axis, 0, 0, tiled=True)


def gathered_copies(x, axis):
    return sent_to_all(x, axis).reshape(-1, *x.shape[1:])


def sent_and_summed(x, axis):
    peers = lax.axis_size(axis)
    parts = lax.all_to_all(x.reshape(peers, -1, *x.shape[1:]), axis, 0, 0, tiled=True)
    return jnp.sum(parts.astype(jnp.float32), axis=0)


LANE = 128


def aligned(width):
    return -(-width // 16) * 16


def packed_rows(hidden):
    return aligned(-(-3 * aligned(hidden) // 2))


def packed(gain, gate, up, down):
    rows, hidden = gate.shape
    block, half = aligned(hidden), packed_rows(hidden)

    def kernel(gain_ref, gate_ref, up_ref, down_ref, out_ref, tall_ref):
        tall_ref[...] = jnp.zeros_like(tall_ref)
        tall_ref[:hidden, :] = gate_ref[...].T * gain_ref[...]
        tall_ref[block : block + hidden, :] = up_ref[...].T * gain_ref[...]
        tall_ref[2 * block : 2 * block + hidden, :] = down_ref[...].T
        halves = (tall_ref[:half, :], tall_ref[half:, :])
        out_ref[...] = jnp.concatenate(halves, axis=1).astype(jnp.bfloat16)

    return pl.pallas_call(
        kernel,
        out_shape=jax.ShapeDtypeStruct((half, 2 * rows), jnp.bfloat16),
        scratch_shapes=[pltpu.VMEM((2 * half, rows), jnp.float32)],
    )(gain[None, :], gate, up, down.T)


def swapped(own):
    ring = lax.axis_size(FS[:2])
    half = own.shape[0] // 2
    low = lax.ppermute(own[:half], FS[:2], [(i, (i - 1) % ring) for i in range(ring)])
    high = lax.ppermute(own[half:], FS[:2], [(i, (i + 1) % ring) for i in range(ring)])
    return own, low, high


def blocks_of(parity, own, low, high, half):
    pairs = own.shape[0] // (2 * half)
    for at in range(pairs):
        where = low if at < pairs // 2 else high
        for ref, row, slot in ((own, at, parity), (where, at % (pairs // 2), 1 - parity)):
            first = ref[2 * row * half : (2 * row + 1) * half, :]
            second = ref[(2 * row + 1) * half : (2 * row + 2) * half, :]
            side = first.shape[1] // 2
            top = jnp.concatenate((first[:, :side], second[:, :side]), axis=1)
            low_part = jnp.concatenate((first[:, side:], second[:, side:]), axis=1)
            spot = pl.ds(pl.multiple_of((2 * at + slot) * LANE, LANE), LANE)
            yield spot, top, low_part


def mixed_part(parity, slabs, full, hidden):
    features, tokens = full.shape
    block, half = aligned(hidden), packed_rows(hidden)

    def kernel(parity_ref, own_ref, low_ref, high_ref, full_ref, out_ref, down_ref):
        squares = jnp.zeros((1, tokens), jnp.float32)
        total = jnp.zeros((2 * block, tokens), jnp.float32)
        spots = []
        for spot, top, rest in blocks_of(parity_ref[0], own_ref, low_ref, high_ref, half):
            piece = full_ref[spot, :]
            wide = piece.astype(jnp.float32)
            squares += jnp.sum(wide * wide, axis=0, keepdims=True)
            total += jnp.dot(
                jnp.concatenate((top, rest[: 2 * block - half]), axis=0),
                piece,
                preferred_element_type=jnp.float32,
            )
            at = len(spots) * LANE
            down_ref[:, at : at + LANE] = rest[2 * block - half : 3 * block - half]
            spots.append(spot)
        total *= lax.rsqrt(squares / features + norm_epsilon)
        gate = total[:block]
        hidden_value = gate / (1.0 + jnp.exp(-gate)) * total[block:]
        hidden_value = hidden_value.T.astype(jnp.bfloat16)
        for at in range(0, len(spots), 2):
            part = jnp.dot(
                hidden_value,
                down_ref[:, at * LANE : (at + 2) * LANE],
                preferred_element_type=jnp.float32,
            )
            for i in range(2):
                out_ref[spots[at + i], :] = part[:, i * LANE : (i + 1) * LANE].T.astype(jnp.bfloat16)

    vmem = pl.BlockSpec(memory_space=pltpu.VMEM)
    return pl.pallas_call(
        kernel,
        in_specs=[pl.BlockSpec(memory_space=pltpu.SMEM)] + [vmem] * (len(slabs) + 1),
        out_specs=vmem,
        out_shape=jax.ShapeDtypeStruct((features, tokens), jnp.bfloat16),
        scratch_shapes=[pltpu.VMEM((block, features), jnp.bfloat16)],
    )(parity, *slabs, full)


def sampler_slabs(parity, slabs, hidden, features):
    block, half = aligned(hidden), packed_rows(hidden)

    def kernel(parity_ref, own_ref, low_ref, high_ref, gate_ref, up_ref, down_ref):
        split = half - block
        for spot, top, rest in blocks_of(parity_ref[0], own_ref, low_ref, high_ref, half):
            gate_ref[:, spot] = top[:hidden]
            up_ref[:split, spot] = top[block:]
            up_ref[split:, spot] = rest[: hidden - split]
            start = 2 * block - half
            down_ref[:, spot] = rest[start : start + hidden]

    vmem = pl.BlockSpec(memory_space=pltpu.VMEM)
    shape = jax.ShapeDtypeStruct((hidden, features), jnp.bfloat16)
    return pl.pallas_call(
        kernel,
        in_specs=[pl.BlockSpec(memory_space=pltpu.SMEM)] + [vmem] * len(slabs),
        out_specs=[vmem] * 3,
        out_shape=[shape] * 3,
    )(parity, *slabs)


def on_device(
    tokens,
    first_gain,
    first_gate,
    first_up,
    first_down,
    first_post,
    second_gain,
    second_gate,
    second_up,
    second_down,
    second_post,
):
    columns = tokens.shape[1]
    hidden = first_gate.shape[1]
    column_start = lax.axis_index(TP) * columns
    full = gathered_copies(tokens.T, TP)
    parity = lax.axis_index("parity").astype(jnp.int32).reshape(1)
    rows_one = packed(first_gain, first_gate, first_up, first_down)
    own_one = lax.all_gather(rows_one, ("pair", "core"), axis=0, tiled=True)
    rows_two = packed(second_gain, second_gate, second_up, second_down)
    own_two = lax.all_gather(rows_two, ("pair", "core"), axis=0, tiled=True)
    slabs_one = swapped(own_one)
    slabs_two = swapped(own_two)
    features = full.shape[0]
    gate_one, up_one, down_one = sampler_slabs(parity, slabs_one, hidden, features)
    gate_two, up_two, down_two = sampler_slabs(parity, slabs_two, hidden, features)

    partial_value = mixed_part(parity, slabs_one, full, hidden)
    share = lax.optimization_barrier(sent_and_summed(partial_value, TP))
    branch = gathered_copies(share.astype(jnp.bfloat16), TP).astype(jnp.float32)
    scale = lax.rsqrt(jnp.mean(branch * branch, axis=0, keepdims=True) + norm_epsilon)
    middle = (full.astype(jnp.float32) + 0.5 * branch * scale * first_post[:, None]).astype(jnp.bfloat16)

    partial_value = mixed_part(parity, slabs_two, middle, hidden)
    share = sent_and_summed(partial_value, TP)
    squares = sent_to_all(jnp.sum(share * share, axis=0, keepdims=True), TP).sum(axis=0)
    scale = lax.rsqrt(squares / middle.shape[0] + norm_epsilon)
    gain_part = lax.dynamic_slice_in_dim(second_post, column_start, columns, 0)
    own = lax.dynamic_slice_in_dim(middle, column_start, columns, 0)
    mixed = (own.astype(jnp.float32) + 0.5 * share * scale * gain_part[:, None]).astype(jnp.bfloat16)
    return (mixed.T, gate_one.T, up_one.T, down_one, gate_two.T, up_two.T, down_two)


def solution(mesh):
    torus = Mesh(mesh.devices.reshape(-1, 2, 2, 8, 4), (*FS, *TP))
    in_specs = (
        P(FS, TP),
        P(FS),
        P(FS, TP),
        P(FS, TP),
        P(TP, FS),
        P(),
        P(FS),
        P(FS, TP),
        P(FS, TP),
        P(TP, FS),
        P(),
    )
    out_specs = (
        P(FS, TP),
        P(None, TP),
        P(None, TP),
        P(TP, None),
        P(None, TP),
        P(None, TP),
        P(TP, None),
    )

    return jax.shard_map(on_device, mesh=torus, in_specs=in_specs, out_specs=out_specs, check_vma=False)
```

time: 233 us -> 205 us (0.88)
  Pallas kernels: 0 us -> 18.3 us
  local copies, waits for them, and re-layouts: 22.1 us -> 8.2 us
  blocking collectives: 63.4 us -> 50.5 us
  matrix products: 10.3 us -> 0 us
  waiting for transfers between devices: 80.2 us -> 70.3 us
  starting transfers between devices: 34 us -> 39.6 us
  other arithmetic: 7.83 us -> 3.06 us
    all_gather x2 -> x0, blocking collectives: 36.6 us -> none  [whole_of(): nearer = lax.all_gather(x, axes[-1], axis=dim, tiled=True)]
    all_to_all x1 -> x2, blocking collectives: 26.9 us -> 50.5 us  [sent_and_summed(): lax.all_to_all(x.reshape(peers, -1, *x.shape[1:]), axis, 0, 0, tiled=True)]
    pallas_call x0 -> x6, Pallas kernels: none -> 18.3 us  [the longest x2 7.51 us: mixed_part(): pl.pallas_call(kernel, in_specs=[pl.BlockSpec(memory_space=pltpu.SMEM)] +...]
    ppermute x0 -> x4, waiting for transfers between devices: none -> 17.4 us  [the longest x2 10.8 us: swapped(): lax.ppermute(own[:half], FS[:2], [(i, (i - 1) % ring) for i in range(ring)])]
    ppermute x0 -> x4, starting transfers between devices: none -> 11.7 us  [the longest x2 6.04 us: swapped(): lax.ppermute(own[half:], FS[:2], [(i, (i + 1) % ring) for i in range(ring)])]
    dot_general x4 -> x0, matrix products: 10.3 us -> none  [the longest x2 6.85 us: partial_mix(): return jnp.dot(hidden, slabs[2], preferred_element_type=jnp.float32)]
    all_gather x2, waiting for transfers between devices: 53.6 us -> 43.7 us  [the longest x1 43.6 us: on_device(): own_one = lax.all_gather(rows_one, ('pair', 'core'), axis=0, tiled=True)]
    all_to_all x1 -> x0, waiting for transfers between devices: 8.74 us -> none  [sent_and_summed(): parts = lax.all_to_all(cut_along(x, dim, peers), axis, 0, 0, tiled=True)]
  transfers between devices with their start and end apart: 6 -> 9, of which waited for: 4 -> 6; matrix products, arithmetic and copies ran while one was open for 12% -> 4% of each run, Pallas kernels for 0% -> 6%
where the time goes in v1:
time: 205 us; the launch traced here: 204 us
  waiting for transfers between devices  70.3 us (34%)
  blocking collectives  50.5 us (25%)
  starting transfers between devices  39.6 us (19%)
  Pallas kernels  18.3 us (9%)
  between operations  14.2 us (7%)
  local copies, waits for them, and re-layouts  8.2 us (4%)
  other arithmetic  3.06 us (1%)
    all_to_all x2, blocking collectives, sent_and_summed(): lax.all_to_all(x.reshape(peers, -1, *x.shape[1:]), axis, 0, 0, tiled=True)  50.5 us
    all_gather x1, waiting for transfers between devices, on_device(): own_one = lax.all_gather(rows_one, ('pair', 'core'), axis=0, tiled=True)  43.6 us
    all_to_all x3, starting transfers between devices, sent_to_all(): lax.all_to_all(jnp.broadcast_to(x[None], (peers, *x.shape)), axis, 0, 0,...  27.8 us
    ppermute x2, waiting for transfers between devices, swapped(): lax.ppermute(own[:half], FS[:2], [(i, (i - 1) % ring) for i in range(ring)])  10.8 us
    all_to_all x3, waiting for transfers between devices, sent_to_all(): lax.all_to_all(jnp.broadcast_to(x[None], (peers, *x.shape)), axis, 0, 0,...  9.27 us
    pallas_call x2, Pallas kernels, mixed_part(): pl.pallas_call(kernel, in_specs=[pl.BlockSpec(memory_space=pltpu.SMEM)] +...  7.51 us
    pallas_call x2, Pallas kernels, sampler_slabs(): pl.pallas_call(kernel, in_specs=[pl.BlockSpec(memory_space=pltpu.SMEM)] +...  7.15 us
    ppermute x2, waiting for transfers between devices, swapped(): lax.ppermute(own[half:], FS[:2], [(i, (i + 1) % ring) for i in range(ring)])  6.61 us
  transfers between devices with their start and end apart: 9, of which 6 were waited for; matrix products, arithmetic and copies ran while one was open for 4% of the time, Pallas kernels for 6%

profile of v1, /device:TPU:2, one launch (start us, length us, event | category | flops | bytes accessed | tf_op | source)
XLA Modules:
  0.0 204.1 jit_solution(5835775441794433779)
XLA Ops:
  7.2 1.8 shard_map.162
  9.0 1.6 broadcast_in_dim.10
  10.7 16.7 %all-to-all-start = ((bf16[32,64,128]{2,1,0:T(8,128)(2,1)}), bf16[32,64,128]{2,1,0:T(8,128)(2,1)S(1)}, u32[]{:S(2)}, u32[]{:S(2)}) async-start(bf16[32,64,128]{2,1,0:T(8,128)(2,1)} %broadcast_in_dim.10), calls=%async_computation | async-start | bytes 1048576 | tf_op jit(solution)/shard_map/all_to_all | solution.py:19
  27.4 1.8 shard_map.164
  29.3 43.6 %all-gather.3.cloned.1.call-done.own_ref = bf16[4352,128]{1,0:T(8,128)(2,1)} async-done(((bf16[272,128]{1,0:T(8,128)(2,1)}), bf16[4352,128]{1,0:T(8,128)(2,1)}) %all-gather.3.cloned.1.call-update) | async-done | bytes 1114128 | tf_op jit(solution)/shard_map/all_gather | solution.py:168
  72.9 1.3 fusion.4
  74.2 3.7 %collective-permute-start = (bf16[2176,128]{1,0:T(8,128)(2,1)S(1)}, bf16[2176,128]{1,0:T(8,128)(2,1)S(1)}, u32[]{:S(2)}, u32[]{:S(2)}) collective-permute-start(bf16[2176,128]{1,0:T(8,128)(2,1)S(1)} %get-tuple-element.20), channel_id=1, source_target_pairs={{0,960},{64,0},{128,64},{192,128},{256,192},{320,256},{384,320},{4... | collective-permute-start | bytes 1671176 | tf_op jit(solution)/shard_map/ppermute | solution.py:65
  77.9 2.1 %collective-permute-start.1 = (bf16[2176,128]{1,0:T(8,128)(2,1)S(1)}, bf16[2176,128]{1,0:T(8,128)(2,1)S(1)}, u32[]{:S(2)}, u32[]{:S(2)}) collective-permute-start(bf16[2176,128]{1,0:T(8,128)(2,1)S(1)} %get-tuple-element.19), channel_id=1, source_target_pairs={{0,64},{64,128},{128,192},{192,256},{256,320},{320,384},{384,448},... | collective-permute-start | bytes 1671176 | tf_op jit(solution)/shard_map/ppermute | solution.py:66
  80.1 10.8 %collective-permute-done.low_ref = bf16[2176,128]{1,0:T(8,128)(2,1)S(1)} collective-permute-done((bf16[2176,128]{1,0:T(8,128)(2,1)S(1)}, bf16[2176,128]{1,0:T(8,128)(2,1)S(1)}, u32[]{:S(2)}, u32[]{:S(2)}) %collective-permute-start) | collective-permute-done | bytes 557088 | tf_op jit(solution)/shard_map/ppermute | solution.py:65
  90.9 4.7 %collective-permute-done.1.high_ref = bf16[2176,128]{1,0:T(8,128)(2,1)S(1)} collective-permute-done((bf16[2176,128]{1,0:T(8,128)(2,1)S(1)}, bf16[2176,128]{1,0:T(8,128)(2,1)S(1)}, u32[]{:S(2)}, u32[]{:S(2)}) %collective-permute-start.1) | collective-permute-done | bytes 557088 | tf_op jit(solution)/shard_map/ppermute | solution.py:66
  95.5 0.8 copy-done.3
  96.3 3.8 %shard_map.163 = bf16[2048,128]{1,0:T(8,128)(2,1)} custom-call(s32[1]{0:T(128)} %bitcast.2.parity_ref, bf16[4352,128]{1,0:T(8,128)(2,1)} %all-gather.3.cloned.1.call-done.own_ref, bf16[2176,128]{1,0:T(8,128)(2,1)} %copy-done.2, bf16[2176,128]{1,0:T(8,128)(2,1)} %copy-done.3, bf16[2048,128]{1,0:T(8,128)(2,1)} %bitcast.25), custom_call_target="tpu_custom_call" | custom-call | tf_op jit(solution)/shard_map/pallas_call | solution.py:118
  100.1 26.1 %all_to_all.25 = bf16[32,64,128]{2,1,0:T(8,128)(2,1)S(1)} all-to-all(bf16[32,64,128]{2,1,0:T(8,128)(2,1)} %bitcast.26), channel_id=1, replica_groups=mesh['pair'=8,'parity'=2,'core'=2,'tp_0'=8,'tp_1'=4] {'tp_0','tp_1'}, dimensions={0} | all-to-all | bytes 1048576 | tf_op jit(solution)/shard_map/all_to_all | solution.py:28
  126.3 0.9 broadcast_in_dim.12
  127.2 5.6 %all-to-all-start.2 = ((bf16[32,64,128]{2,1,0:T(8,128)(2,1)}), bf16[32,64,128]{2,1,0:T(8,128)(2,1)S(1)}, u32[]{:S(2)}, u32[]{:S(2)}) async-start(bf16[32,64,128]{2,1,0:T(8,128)(2,1)} %broadcast_in_dim.12), calls=%async_computation.2 | async-start | bytes 1048576 | tf_op jit(solution)/shard_map/all_to_all | solution.py:19
  132.8 1.3 fusion.5
  134.2 1.9 collective-permute-start.2
  136.1 3.9 %collective-permute-start.3 = (bf16[2176,128]{1,0:T(8,128)(2,1)S(1)}, bf16[2176,128]{1,0:T(8,128)(2,1)S(1)}, u32[]{:S(2)}, u32[]{:S(2)}) collective-permute-start(bf16[2176,128]{1,0:T(8,128)(2,1)S(1)} %get-tuple-element.21), channel_id=1, source_target_pairs={{0,64},{64,128},{128,192},{192,256},{256,320},{320,384},{384,448},... | collective-permute-start | bytes 1671176 | tf_op jit(solution)/shard_map/ppermute | solution.py:66
  140.0 8.7 %all-to-all-done.2 = bf16[32,64,128]{2,1,0:T(8,128)(2,1)S(1)} async-done(((bf16[32,64,128]{2,1,0:T(8,128)(2,1)}), bf16[32,64,128]{2,1,0:T(8,128)(2,1)S(1)}, u32[]{:S(2)}, u32[]{:S(2)}) %all-to-all-start.2) | async-done | bytes 524320 | tf_op jit(solution)/shard_map/all_to_all | solution.py:19
  148.8 0.3 multiply_reduce_fusion
  149.1 1.1 fusion.2.full_ref
  150.2 2.0 collective-permute-done.3.high_ref
  152.2 0.8 copy-done.5
  153.0 3.8 %shard_map.165 = bf16[2048,128]{1,0:T(8,128)(2,1)} custom-call(s32[1]{0:T(128)} %bitcast.2.parity_ref, bf16[4352,128]{1,0:T(8,128)(2,1)} %all-gather.5.cloned.1.call-done.own_ref, bf16[2176,128]{1,0:T(8,128)(2,1)} %copy-done.4, bf16[2176,128]{1,0:T(8,128)(2,1)} %copy-done.5, bf16[2048,128]{1,0:T(8,128)(2,1)} %fusion.2.full_ref), custom_call_target="tpu_custom_call" | custom-call | tf_op jit(solution)/shard_map/pallas_call | solution.py:118
  156.7 24.3 %all_to_all.26 = bf16[32,64,128]{2,1,0:T(8,128)(2,1)S(1)} all-to-all(bf16[32,64,128]{2,1,0:T(8,128)(2,1)} %bitcast.27), channel_id=1, replica_groups=mesh['pair'=8,'parity'=2,'core'=2,'tp_0'=8,'tp_1'=4] {'tp_0','tp_1'}, dimensions={0} | all-to-all | bytes 1048576 | tf_op jit(solution)/shard_map/all_to_all | solution.py:28
  181.2 0.6 broadcast_in_dim.14
  181.8 5.6 %all-to-all-start.4 = ((f32[32,1,128]{2,1,0:T(1,128)}), f32[32,1,128]{2,1,0:T(1,128)S(1)}, u32[]{:S(2)}, u32[]{:S(2)}) async-start(f32[32,1,128]{2,1,0:T(1,128)} %broadcast_in_dim.14), calls=%async_computation.4 | async-start | bytes 32768 | tf_op jit(solution)/shard_map/all_to_all | solution.py:19
  187.4 0.8 dynamic_slice.7
  188.1 3.6 %shard_map.166 = (bf16[172,2048]{1,0:T(8,128)(2,1)}, bf16[172,2048]{1,0:T(8,128)(2,1)}, bf16[172,2048]{1,0:T(8,128)(2,1)}) custom-call(s32[1]{0:T(128)} %bitcast.2.parity_ref, bf16[4352,128]{1,0:T(8,128)(2,1)} %all-gather.3.cloned.1.call-done.own_ref, bf16[2176,128]{1,0:T(8,128)(2,1)} %copy-done.2, bf16[2176,128]{1,0:T(8,128)(2,1)} %copy-done.3), custom_call_target="tpu_custom_call" | custom-call | tf_op jit(solution)/shard_map/pallas_call | solution.py:141
  191.7 3.6 %shard_map.167 = (bf16[172,2048]{1,0:T(8,128)(2,1)}, bf16[172,2048]{1,0:T(8,128)(2,1)}, bf16[172,2048]{1,0:T(8,128)(2,1)}) custom-call(s32[1]{0:T(128)} %bitcast.2.parity_ref, bf16[4352,128]{1,0:T(8,128)(2,1)} %all-gather.5.cloned.1.call-done.own_ref, bf16[2176,128]{1,0:T(8,128)(2,1)} %copy-done.4, bf16[2176,128]{1,0:T(8,128)(2,1)} %copy-done.5), custom_call_target="tpu_custom_call" | custom-call | tf_op jit(solution)/shard_map/pallas_call | solution.py:141
  195.3 0.6 all-to-all-done.4
  195.9 1.4 fusion.3
  (25 shorter events, 0.4 us)
Async XLA Ops:
  7.2 65.7 %all-gather.3.cloned.1.call-start = ((), (), s32[]{:S(2)}) async-start(), calls=%async_computation.5 | async-start | bytes 1183744 | tf_op jit(solution)/shard_map/all_gather | solution.py:168
  10.7 69.4 %all-to-all-start = ((bf16[32,64,128]{2,1,0:T(8,128)(2,1)}), bf16[32,64,128]{2,1,0:T(8,128)(2,1)S(1)}, u32[]{:S(2)}, u32[]{:S(2)}) async-start(bf16[32,64,128]{2,1,0:T(8,128)(2,1)} %broadcast_in_dim.10), calls=%async_computation | async-start | bytes 1048576 | tf_op jit(solution)/shard_map/all_to_all | solution.py:19
  27.4 105.4 %all-gather.5.cloned.1.call-start = ((), (), s32[]{:S(2)}) async-start(), calls=%async_computation.6 | async-start | bytes 1183744 | tf_op jit(solution)/shard_map/all_gather | solution.py:170
  74.2 16.6 %collective-permute-start = (bf16[2176,128]{1,0:T(8,128)(2,1)S(1)}, bf16[2176,128]{1,0:T(8,128)(2,1)S(1)}, u32[]{:S(2)}, u32[]{:S(2)}) collective-permute-start(bf16[2176,128]{1,0:T(8,128)(2,1)S(1)} %get-tuple-element.20), channel_id=1, source_target_pairs={{0,960},{64,0},{128,64},{192,128},{256,192},{320,256},{384,320},{4... | collective-permute-start | bytes 1671176 | tf_op jit(solution)/shard_map/ppermute | solution.py:65
  77.9 17.6 %collective-permute-start.1 = (bf16[2176,128]{1,0:T(8,128)(2,1)S(1)}, bf16[2176,128]{1,0:T(8,128)(2,1)S(1)}, u32[]{:S(2)}, u32[]{:S(2)}) collective-permute-start(bf16[2176,128]{1,0:T(8,128)(2,1)S(1)} %get-tuple-element.19), channel_id=1, source_target_pairs={{0,64},{64,128},{128,192},{192,256},{256,320},{320,384},{384,448},... | collective-permute-start | bytes 1671176 | tf_op jit(solution)/shard_map/ppermute | solution.py:66
  80.1 15.4 %copy-start = (bf16[32,64,128]{2,1,0:T(8,128)(2,1)}, bf16[32,64,128]{2,1,0:T(8,128)(2,1)S(1)}, u32[]{:S(2)}) copy-start(bf16[32,64,128]{2,1,0:T(8,128)(2,1)S(1)} %all-to-all-done) | copy-start | bytes 1572868
  90.8 4.7 %copy-start.2 = (bf16[2176,128]{1,0:T(8,128)(2,1)}, bf16[2176,128]{1,0:T(8,128)(2,1)S(1)}, u32[]{:S(2)}) copy-start(bf16[2176,128]{1,0:T(8,128)(2,1)S(1)} %collective-permute-done.low_ref) | copy-start | bytes 1671172
  95.5 0.8 copy-start.3
  127.2 21.5 %all-to-all-start.2 = ((bf16[32,64,128]{2,1,0:T(8,128)(2,1)}), bf16[32,64,128]{2,1,0:T(8,128)(2,1)S(1)}, u32[]{:S(2)}, u32[]{:S(2)}) async-start(bf16[32,64,128]{2,1,0:T(8,128)(2,1)} %broadcast_in_dim.12), calls=%async_computation.2 | async-start | bytes 1048576 | tf_op jit(solution)/shard_map/all_to_all | solution.py:19
  132.8 16.3 %copy-start.1 = (bf16[32,64,128]{2,1,0:T(8,128)(2,1)S(1)}, bf16[32,64,128]{2,1,0:T(8,128)(2,1)}, u32[]{:S(2)}) copy-start(bf16[32,64,128]{2,1,0:T(8,128)(2,1)} %copy-done) | copy-start | bytes 1572868
  132.8 16.3 %copy-start.6 = (f32[2048]{0:T(1024)S(1)}, f32[2048]{0:T(1024)}, u32[]{:S(2)}) copy-start(f32[2048]{0:T(1024)} %param.16) | copy-start | bytes 24580
  134.2 16.0 %collective-permute-start.2 = (bf16[2176,128]{1,0:T(8,128)(2,1)S(1)}, bf16[2176,128]{1,0:T(8,128)(2,1)S(1)}, u32[]{:S(2)}, u32[]{:S(2)}) collective-permute-start(bf16[2176,128]{1,0:T(8,128)(2,1)S(1)} %get-tuple-element.22), channel_id=1, source_target_pairs={{0,960},{64,0},{128,64},{192,128},{256,192},{320,256},{384,320},{4... | collective-permute-start | bytes 1671176 | tf_op jit(solution)/shard_map/ppermute | solution.py:65
  136.1 16.1 %collective-permute-start.3 = (bf16[2176,128]{1,0:T(8,128)(2,1)S(1)}, bf16[2176,128]{1,0:T(8,128)(2,1)S(1)}, u32[]{:S(2)}, u32[]{:S(2)}) collective-permute-start(bf16[2176,128]{1,0:T(8,128)(2,1)S(1)} %get-tuple-element.21), channel_id=1, source_target_pairs={{0,64},{64,128},{128,192},{192,256},{256,320},{320,384},{384,448},... | collective-permute-start | bytes 1671176 | tf_op jit(solution)/shard_map/ppermute | solution.py:66
  150.2 2.0 copy-start.4
  152.2 0.8 copy-start.5
  181.8 14.1 %all-to-all-start.4 = ((f32[32,1,128]{2,1,0:T(1,128)}), f32[32,1,128]{2,1,0:T(1,128)S(1)}, u32[]{:S(2)}, u32[]{:S(2)}) async-start(f32[32,1,128]{2,1,0:T(1,128)} %broadcast_in_dim.14), calls=%async_computation.4 | async-start | bytes 32768 | tf_op jit(solution)/shard_map/all_to_all | solution.py:19
Sparse Core Ops, SparseCore 0:
  11.3 61.6 all-gather.2
  76.2 49.3 all-gather.4

commit v2 on v1

--- a/solution.py
+++ b/solution.py
@@ -59,38 +59,67 @@
     )(gain[None, :], gate, up, down.T)
 
 
-def swapped(own):
+def from_neighbours(own):
     ring = lax.axis_size(FS[:2])
     half = own.shape[0] // 2
     low = lax.ppermute(own[:half], FS[:2], [(i, (i - 1) % ring) for i in range(ring)])
     high = lax.ppermute(own[half:], FS[:2], [(i, (i + 1) % ring) for i in range(ring)])
-    return own, low, high
-
-
-def blocks_of(parity, own, low, high, half):
-    pairs = own.shape[0] // (2 * half)
+    return low, high
+
+
+def from_partner(x):
+    return lax.ppermute(x, "core", [(0, 1), (1, 0)])
+
+
+def blocks_of(place_ref, refs, half):
+    parity, core = place_ref[0], place_ref[1]
+    alone = len(refs) == 6
+    pairs = refs[0].shape[0] // half // (1 if alone else 2)
     for at in range(pairs):
-        where = low if at < pairs // 2 else high
-        for ref, row, slot in ((own, at, parity), (where, at % (pairs // 2), 1 - parity)):
-            first = ref[2 * row * half : (2 * row + 1) * half, :]
-            second = ref[(2 * row + 1) * half : (2 * row + 2) * half, :]
-            side = first.shape[1] // 2
-            top = jnp.concatenate((first[:, :side], second[:, :side]), axis=1)
-            low_part = jnp.concatenate((first[:, side:], second[:, side:]), axis=1)
-            spot = pl.ds(pl.multiple_of((2 * at + slot) * LANE, LANE), LANE)
-            yield spot, top, low_part
-
-
-def mixed_part(parity, slabs, full, hidden):
+        late = at >= pairs // 2
+        row = at % (pairs // 2)
+        if alone:
+            own, mate, low, high, mate_low, mate_high = refs
+            sides = (
+                (parity, own, at, mate, at),
+                (1 - parity, high if late else low, row, mate_high if late else mate_low, row),
+            )
+            cores = (core, 1 - core)
+        else:
+            own, low, high = refs
+            other = high if late else low
+            sides = (
+                (parity, own, 2 * at, own, 2 * at + 1),
+                (1 - parity, other, 2 * row, other, 2 * row + 1),
+            )
+            cores = (0, 1)
+        for slot, one, one_row, two, two_row in sides:
+            first = one[one_row * half : (one_row + 1) * half, :]
+            second = two[two_row * half : (two_row + 1) * half, :]
+            yield 2 * at + slot, cores, first, second
+
+
+def joined(first, second):
+    side = first.shape[1] // 2
+    top = jnp.concatenate((first[:, :side], second[:, :side]), axis=1)
+    rest = jnp.concatenate((first[:, side:], second[:, side:]), axis=1)
+    return top, rest
+
+
+def mixed_part(place, slabs, full, hidden):
     features, tokens = full.shape
     block, half = aligned(hidden), packed_rows(hidden)
-
-    def kernel(parity_ref, own_ref, low_ref, high_ref, full_ref, out_ref, down_ref):
+    side = LANE // 2
+
+    def kernel(place_ref, *refs):
+        *slab_refs, full_ref, out_ref, down_ref = refs
         squares = jnp.zeros((1, tokens), jnp.float32)
         total = jnp.zeros((2 * block, tokens), jnp.float32)
         spots = []
-        for spot, top, rest in blocks_of(parity_ref[0], own_ref, low_ref, high_ref, half):
-            piece = full_ref[spot, :]
+        for spot, cores, first, second in blocks_of(place_ref, slab_refs, half):
+            spot = [pl.ds(pl.multiple_of(spot * LANE + core * side, side), side) for core in cores]
+            top, rest = joined(first, second)
+            piece = jnp.concatenate([full_ref[rows, :] for rows in spot], axis=0)
             wide = piece.astype(jnp.float32)
             squares += jnp.sum(wide * wide, axis=0, keepdims=True)
             total += jnp.dot(
@@ -98,21 +127,21 @@
                 piece,
                 preferred_element_type=jnp.float32,
             )
-            at = len(spots) * LANE
+            at = len(spots) // 2 * LANE
             down_ref[:, at : at + LANE] = rest[2 * block - half : 3 * block - half]
-            spots.append(spot)
+            spots += spot
         total *= lax.rsqrt(squares / features + norm_epsilon)
         gate = total[:block]
         hidden_value = gate / (1.0 + jnp.exp(-gate)) * total[block:]
         hidden_value = hidden_value.T.astype(jnp.bfloat16)
-        for at in range(0, len(spots), 2):
+        for at in range(0, features, 2 * LANE):
             part = jnp.dot(
-                hidden_value,
-                down_ref[:, at * LANE : (at + 2) * LANE],
-                preferred_element_type=jnp.float32,
-            )
-            for i in range(2):
-                out_ref[spots[at + i], :] = part[:, i * LANE : (i + 1) * LANE].T.astype(jnp.bfloat16)
+                hidden_value, down_ref[:, at : at + 2 * LANE], preferred_element_type=jnp.float32
+            )
+            for i in range(0, 2 * LANE, LANE):
+                turned = part[:, i : i + LANE].T.astype(jnp.bfloat16)
+                for j in range(2):
+                    out_ref[spots[(at + i) // side + j], :] = turned[j * side : (j + 1) * side]
 
     vmem = pl.BlockSpec(memory_space=pltpu.VMEM)
     return pl.pallas_call(
@@ -121,15 +150,23 @@
         out_specs=vmem,
         out_shape=jax.ShapeDtypeStruct((features, tokens), jnp.bfloat16),
         scratch_shapes=[pltpu.VMEM((block, features), jnp.bfloat16)],
-    )(parity, *slabs, full)
-
-
-def sampler_slabs(parity, slabs, hidden, features):
+    )(place, *slabs, full)
+
+
+def sampler_slabs(place, slabs, hidden, features):
     block, half = aligned(hidden), packed_rows(hidden)
 
-    def kernel(parity_ref, own_ref, low_ref, high_ref, gate_ref, up_ref, down_ref):
+    def kernel(place_ref, *refs):
+        *slab_refs, gate_ref, up_ref, down_ref = refs
         split = half - block
-        for spot, top, rest in blocks_of(parity_ref[0], own_ref, low_ref, high_ref, half):
+        for spot, cores, first, second in blocks_of(place_ref, slab_refs, half):
+            if len(slab_refs) == 6:
+                first, second = (
+                    jnp.where(cores[0] == 0, first, second),
+                    jnp.where(cores[0] == 0, second, first),
+                )
+            top, rest = joined(first, second)
+            spot = pl.ds(pl.multiple_of(spot * LANE, LANE), LANE)
             gate_ref[:, spot] = top[:hidden]
             up_ref[:split, spot] = top[block:]
             up_ref[split:, spot] = rest[: hidden - split]
@@ -143,7 +180,7 @@
         in_specs=[pl.BlockSpec(memory_space=pltpu.SMEM)] + [vmem] * len(slabs),
         out_specs=[vmem] * 3,
         out_shape=[shape] * 3,
-    )(parity, *slabs)
+    )(place, *slabs)
 
 
 def on_device(
@@ -163,30 +200,33 @@
     hidden = first_gate.shape[1]
     column_start = lax.axis_index(TP) * columns
     full = gathered_copies(tokens.T, TP)
-    parity = lax.axis_index("parity").astype(jnp.int32).reshape(1)
+    place = jnp.stack([lax.axis_index("parity"), lax.axis_index("core")]).astype(jnp.int32)
     rows_one = packed(first_gain, first_gate, first_up, first_down)
-    own_one = lax.all_gather(rows_one, ("pair", "core"), axis=0, tiled=True)
     rows_two = packed(second_gain, second_gate, second_up, second_down)
     own_two = lax.all_gather(rows_two, ("pair", "core"), axis=0, tiled=True)
-    slabs_one = swapped(own_one)
-    slabs_two = swapped(own_two)
+    own_one = lax.all_gather(rows_one, "pair", axis=0, tiled=True)
+    near_one = from_neighbours(own_one)
+    mates_one = [from_partner(x) for x in (own_one, *near_one)]
+    slabs_one = (own_one, mates_one[0], *near_one, *mates_one[1:])
+    slabs_two = (own_two, *from_neighbours(own_two))
     features = full.shape[0]
-    gate_one, up_one, down_one = sampler_slabs(parity, slabs_one, hidden, features)
-    gate_two, up_two, down_two = sampler_slabs(parity, slabs_two, hidden, features)
-
-    partial_value = mixed_part(parity, slabs_one, full, hidden)
+    gate_one, up_one, down_one = sampler_slabs(place, slabs_one, hidden, features)
+    gate_two, up_two, down_two = sampler_slabs(place, slabs_two, hidden, features)
+
+    partial_value = mixed_part(place, slabs_one, full, hidden)
     share = lax.optimization_barrier(sent_and_summed(partial_value, TP))
     branch = gathered_copies(share.astype(jnp.bfloat16), TP).astype(jnp.float32)
     scale = lax.rsqrt(jnp.mean(branch * branch, axis=0, keepdims=True) + norm_epsilon)
     middle = (full.astype(jnp.float32) + 0.5 * branch * scale * first_post[:, None]).astype(jnp.bfloat16)
 
-    partial_value = mixed_part(parity, slabs_two, middle, hidden)
+    partial_value = mixed_part(place, slabs_two, middle, hidden)
     share = sent_and_summed(partial_value, TP)
     squares = sent_to_all(jnp.sum(share * share, axis=0, keepdims=True), TP).sum(axis=0)
     scale = lax.rsqrt(squares / middle.shape[0] + norm_epsilon)
     gain_part = lax.dynamic_slice_in_dim(second_post, column_start, columns, 0)
-    own = lax.dynamic_slice_in_dim(middle, column_start, columns, 0)
-    mixed = (own.astype(jnp.float32) + 0.5 * share * scale * gain_part[:, None]).astype(jnp.bfloat16)
+    own = lax.dynamic_slice_in_dim(middle, column_start, columns, 0).astype(jnp.float32)
+    own, moved = lax.optimization_barrier((own, 0.5 * share * gain_part[:, None]))
+    mixed = (own + moved * scale).astype(jnp.bfloat16)
     return (mixed.T, gate_one.T, up_one.T, down_one, gate_two.T, up_two.T, down_two)
 
 

time: 205 us -> 198 us (0.966)
  waiting for transfers between devices: 70.3 us -> 32.4 us
  starting transfers between devices: 39.6 us -> 56.8 us
  blocking collectives: 50.5 us -> 63.9 us
    all_gather x1 -> x0, waiting for transfers between devices: 43.6 us -> none  [on_device(): own_one = lax.all_gather(rows_one, ('pair', 'core'), axis=0, tiled=True)]
    all_gather x0 -> x1, blocking collectives: none -> 37.2 us  [on_device(): own_one = lax.all_gather(rows_one, 'pair', axis=0, tiled=True)]
    all_to_all x2 -> x1, blocking collectives: 50.5 us -> 26.7 us  [sent_and_summed(): lax.all_to_all(x.reshape(peers, -1, *x.shape[1:]), axis, 0, 0, tiled=True)]
    all_to_all x0 -> x1, starting transfers between devices: none -> 9.77 us  [sent_and_summed(): lax.all_to_all(x.reshape(peers, -1, *x.shape[1:]), axis, 0, 0, tiled=True)]
    ppermute x4 -> x7, waiting for transfers between devices: 17.4 us -> 9.45 us  [the longest x2 6.04 us: from_neighbours(): lax.ppermute(own[half:], FS[:2], [(i, (i + 1) % ring) for i in range(ring)])]
    ppermute x4 -> x7, starting transfers between devices: 11.7 us -> 19.2 us  [the longest x2 9.23 us: from_neighbours(): lax.ppermute(own[:half], FS[:2], [(i, (i - 1) % ring) for i in range(ring)])]
    all_to_all x3, waiting for transfers between devices: 9.27 us -> 16.5 us  [sent_to_all(): lax.all_to_all(jnp.broadcast_to(x[None], (peers, *x.shape)), axis, 0, 0,...]
    all_to_all x0 -> x1, waiting for transfers between devices: none -> 6.43 us  [sent_and_summed(): lax.all_to_all(x.reshape(peers, -1, *x.shape[1:]), axis, 0, 0, tiled=True)]
  transfers between devices with their start and end apart: 9 -> 12, of which waited for: 6 -> 7; matrix products, arithmetic and copies ran while one was open for 4% -> 3% of each run, Pallas kernels for 6% -> 7%
where the time goes in v2:
time: 198 us; the launch traced here: 197 us
  blocking collectives  63.9 us (32%)
  starting transfers between devices  56.8 us (29%)
  waiting for transfers between devices  32.4 us (16%)
  Pallas kernels  18.5 us (9%)
  between operations  14.2 us (7%)
  local copies, waits for them, and re-layouts  6.38 us (3%)
  other arithmetic  4.38 us (2%)
    all_gather x1, blocking collectives, on_device(): own_one = lax.all_gather(rows_one, 'pair', axis=0, tiled=True)  37.2 us
    all_to_all x3, starting transfers between devices, sent_to_all(): lax.all_to_all(jnp.broadcast_to(x[None], (peers, *x.shape)), axis, 0, 0,...  27.8 us
    all_to_all x1, blocking collectives, sent_and_summed(): lax.all_to_all(x.reshape(peers, -1, *x.shape[1:]), axis, 0, 0, tiled=True)  26.7 us
    all_to_all x3, waiting for transfers between devices, sent_to_all(): lax.all_to_all(jnp.broadcast_to(x[None], (peers, *x.shape)), axis, 0, 0,...  16.5 us
    all_to_all x1, starting transfers between devices, sent_and_summed(): lax.all_to_all(x.reshape(peers, -1, *x.shape[1:]), axis, 0, 0, tiled=True)  9.77 us
    ppermute x2, starting transfers between devices, from_neighbours(): lax.ppermute(own[:half], FS[:2], [(i, (i - 1) % ring) for i in range(ring)])  9.23 us
    pallas_call x2, Pallas kernels, mixed_part(): pl.pallas_call(kernel, in_specs=[pl.BlockSpec(memory_space=pltpu.SMEM)] +...  7.56 us
    pallas_call x2, Pallas kernels, sampler_slabs(): pl.pallas_call(kernel, in_specs=[pl.BlockSpec(memory_space=pltpu.SMEM)] +...  7.29 us
  transfers between devices with their start and end apart: 12, of which 7 were waited for; matrix products, arithmetic and copies ran while one was open for 3% of the time, Pallas kernels for 7%

profile of v2, /device:TPU:2, one launch (start us, length us, event | category | flops | bytes accessed | tf_op | source)
XLA Modules:
  0.0 196.5 jit_solution(15371238267081478205)
XLA Ops:
  7.2 1.6 broadcast_in_dim.10
  8.8 16.7 %all-to-all-start = ((bf16[32,64,128]{2,1,0:T(8,128)(2,1)}), bf16[32,64,128]{2,1,0:T(8,128)(2,1)S(1)}, u32[]{:S(2)}, u32[]{:S(2)}) async-start(bf16[32,64,128]{2,1,0:T(8,128)(2,1)} %broadcast_in_dim.10), calls=%async_computation | async-start | bytes 1048576 | tf_op jit(solution)/shard_map/all_to_all | solution.py:19
  25.6 1.8 shard_map.164
  27.4 1.8 shard_map.162
  29.2 37.2 %all_gather.6.refs_0_ = bf16[2176,128]{1,0:T(8,128)(2,1)S(1)} all-gather(bf16[272,128]{1,0:T(8,128)(2,1)} %shard_map.162), channel_id=1, replica_groups=mesh['pair'=8,'parity'=2,'core'=2,'tp_0'=8,'tp_1'=4] {'pair'}, dimensions={0}, use_global_device_ids=true | all-gather | bytes 626688 | tf_op jit(solution)/shard_map/all_gather | solution.py:207
  66.4 5.7 %collective-permute-start.1 = (bf16[1088,128]{1,0:T(8,128)(2,1)S(1)}, bf16[1088,128]{1,0:T(8,128)(2,1)S(1)}, u32[]{:S(2)}, u32[]{:S(2)}) collective-permute-start(bf16[1088,128]{1,0:T(8,128)(2,1)S(1)} %get-tuple-element.26), channel_id=1, source_target_pairs={{0,960},{64,0},{128,64},{192,128},{256,192},{320,256},{384,320},{4... | collective-permute-start | bytes 835592 | tf_op jit(solution)/shard_map/ppermute | solution.py:65
  72.1 1.9 collective-permute-start.2
  74.0 1.9 collective-permute-start
  76.0 2.5 %collective-permute-done.1.refs_2_ = bf16[1088,128]{1,0:T(8,128)(2,1)S(1)} collective-permute-done((bf16[1088,128]{1,0:T(8,128)(2,1)S(1)}, bf16[1088,128]{1,0:T(8,128)(2,1)S(1)}, u32[]{:S(2)}, u32[]{:S(2)}) %collective-permute-start.1) | collective-permute-done | bytes 278560 | tf_op jit(solution)/shard_map/ppermute | solution.py:65
  78.4 1.9 collective-permute-start.3
  80.3 2.5 %collective-permute-done.2.refs_3_ = bf16[1088,128]{1,0:T(8,128)(2,1)S(1)} collective-permute-done((bf16[1088,128]{1,0:T(8,128)(2,1)S(1)}, bf16[1088,128]{1,0:T(8,128)(2,1)S(1)}, u32[]{:S(2)}, u32[]{:S(2)}) %collective-permute-start.2) | collective-permute-done | bytes 278560 | tf_op jit(solution)/shard_map/ppermute | solution.py:66
  82.9 1.9 collective-permute-start.4
  85.4 1.0 collective-permute-done.4.refs_5_
  87.4 3.8 %shard_map.163 = bf16[2048,128]{1,0:T(8,128)(2,1)} custom-call(s32[2]{0:T(128)} %pad_add_fusion.place_ref, bf16[2176,128]{1,0:T(8,128)(2,1)} %copy-done, bf16[2176,128]{1,0:T(8,128)(2,1)} %copy-done.3, bf16[1088,128]{1,0:T(8,128)(2,1)} %copy-done.6, bf16[1088,128]{1,0:T(8,128)(2,1)} %copy-done.7, bf16[1088,128]{1,0:T(8,128)(2,1)} %copy-done.8, ...), custom_call_target="tpu_custom_call" | custom-call | tf_op jit(solution)/shard_map/pallas_call | solution.py:147
  91.2 26.7 %all_to_all.25 = bf16[32,64,128]{2,1,0:T(8,128)(2,1)S(1)} all-to-all(bf16[32,64,128]{2,1,0:T(8,128)(2,1)} %bitcast.28), channel_id=1, replica_groups=mesh['pair'=8,'parity'=2,'core'=2,'tp_0'=8,'tp_1'=4] {'tp_0','tp_1'}, dimensions={0} | all-to-all | bytes 1048576 | tf_op jit(solution)/shard_map/all_to_all | solution.py:28
  118.0 0.9 broadcast_in_dim.12
  118.9 5.6 %all-to-all-start.2 = ((bf16[32,64,128]{2,1,0:T(8,128)(2,1)}), bf16[32,64,128]{2,1,0:T(8,128)(2,1)S(1)}, u32[]{:S(2)}, u32[]{:S(2)}) async-start(bf16[32,64,128]{2,1,0:T(8,128)(2,1)} %broadcast_in_dim.12), calls=%async_computation.2 | async-start | bytes 1048576 | tf_op jit(solution)/shard_map/all_to_all | solution.py:19
  124.5 1.3 fusion.4
  125.8 3.5 %collective-permute-start.5 = (bf16[2176,128]{1,0:T(8,128)(2,1)S(1)}, bf16[2176,128]{1,0:T(8,128)(2,1)S(1)}, u32[]{:S(2)}, u32[]{:S(2)}) collective-permute-start(bf16[2176,128]{1,0:T(8,128)(2,1)S(1)} %get-tuple-element.24), channel_id=1, source_target_pairs={{0,960},{64,0},{128,64},{192,128},{256,192},{320,256},{384,320},{4... | collective-permute-start | bytes 1671176 | tf_op jit(solution)/shard_map/ppermute | solution.py:65
  129.4 2.3 %collective-permute-start.6 = (bf16[2176,128]{1,0:T(8,128)(2,1)S(1)}, bf16[2176,128]{1,0:T(8,128)(2,1)S(1)}, u32[]{:S(2)}, u32[]{:S(2)}) collective-permute-start(bf16[2176,128]{1,0:T(8,128)(2,1)S(1)} %get-tuple-element.23), channel_id=1, source_target_pairs={{0,64},{64,128},{128,192},{192,256},{256,320},{320,384},{384,448},... | collective-permute-start | bytes 1671176 | tf_op jit(solution)/shard_map/ppermute | solution.py:66
  131.7 8.7 %all-to-all-done.2 = bf16[32,64,128]{2,1,0:T(8,128)(2,1)S(1)} async-done(((bf16[32,64,128]{2,1,0:T(8,128)(2,1)}), bf16[32,64,128]{2,1,0:T(8,128)(2,1)S(1)}, u32[]{:S(2)}, u32[]{:S(2)}) %all-to-all-start.2) | async-done | bytes 524320 | tf_op jit(solution)/shard_map/all_to_all | solution.py:19
  140.7 1.1 fusion.2.refs_3_
  141.9 3.5 %collective-permute-done.6.refs_2_ = bf16[2176,128]{1,0:T(8,128)(2,1)S(1)} collective-permute-done((bf16[2176,128]{1,0:T(8,128)(2,1)S(1)}, bf16[2176,128]{1,0:T(8,128)(2,1)S(1)}, u32[]{:S(2)}, u32[]{:S(2)}) %collective-permute-start.6) | collective-permute-done | bytes 557088 | tf_op jit(solution)/shard_map/ppermute | solution.py:66
  145.4 0.8 copy-done.5
  146.2 3.8 %shard_map.165 = bf16[2048,128]{1,0:T(8,128)(2,1)} custom-call(s32[2]{0:T(128)} %pad_add_fusion.place_ref, bf16[4352,128]{1,0:T(8,128)(2,1)} %all-gather.2.cloned.1.call-done.refs_0_, bf16[2176,128]{1,0:T(8,128)(2,1)} %copy-done.4, bf16[2176,128]{1,0:T(8,128)(2,1)} %copy-done.5, bf16[2048,128]{1,0:T(8,128)(2,1)} %fusion.2.refs_3_), custom_call_target="tpu_custom_call" | custom-call | tf_op jit(solution)/shard_map/pallas_call | solution.py:147
  149.9 9.8 %all-to-all-start.3 = ((bf16[32,64,128]{2,1,0:T(8,128)(2,1)}), bf16[32,64,128]{2,1,0:T(8,128)(2,1)S(1)}, u32[]{:S(2)}, u32[]{:S(2)}) async-start(bf16[32,64,128]{2,1,0:T(8,128)(2,1)} %bitcast.27), calls=%async_computation.3 | async-start | bytes 1048576 | tf_op jit(solution)/shard_map/all_to_all | solution.py:28
  159.7 0.8 dynamic-slice_multiply_fusion
  160.5 3.7 %shard_map.166 = (bf16[172,2048]{1,0:T(8,128)(2,1)}, bf16[172,2048]{1,0:T(8,128)(2,1)}, bf16[172,2048]{1,0:T(8,128)(2,1)}) custom-call(s32[2]{0:T(128)} %pad_add_fusion.place_ref, bf16[2176,128]{1,0:T(8,128)(2,1)} %copy-done, bf16[2176,128]{1,0:T(8,128)(2,1)} %copy-done.3, bf16[1088,128]{1,0:T(8,128)(2,1)} %copy-done.6, bf16[1088,128]{1,0:T(8,128)(2,1)} %copy-done.7, ...), custom_call_target="tpu_custom_call" | custom-call | tf_op jit(solution)/shard_map/pallas_call | solution.py:178
  164.2 3.6 %shard_map.167 = (bf16[172,2048]{1,0:T(8,128)(2,1)}, bf16[172,2048]{1,0:T(8,128)(2,1)}, bf16[172,2048]{1,0:T(8,128)(2,1)}) custom-call(s32[2]{0:T(128)} %pad_add_fusion.place_ref, bf16[4352,128]{1,0:T(8,128)(2,1)} %all-gather.2.cloned.1.call-done.refs_0_, bf16[2176,128]{1,0:T(8,128)(2,1)} %copy-done.4, bf16[2176,128]{1,0:T(8,128)(2,1)} %copy-done.5), custom_call_target="tpu_custom_call" | custom-call | tf_op jit(solution)/shard_map/pallas_call | solution.py:178
  167.8 6.4 %all-to-all-done.3 = bf16[32,64,128]{2,1,0:T(8,128)(2,1)S(1)} async-done(((bf16[32,64,128]{2,1,0:T(8,128)(2,1)}), bf16[32,64,128]{2,1,0:T(8,128)(2,1)S(1)}, u32[]{:S(2)}, u32[]{:S(2)}) %all-to-all-start.3) | async-done | bytes 524320 | tf_op jit(solution)/shard_map/all_to_all | solution.py:28
  175.0 5.6 %all-to-all-start.4 = ((f32[32,1,128]{2,1,0:T(1,128)}), f32[32,1,128]{2,1,0:T(1,128)S(1)}, u32[]{:S(2)}, u32[]{:S(2)}) async-start(f32[32,1,128]{2,1,0:T(1,128)} %broadcast_in_dim.14), calls=%async_computation.4 | async-start | bytes 32768 | tf_op jit(solution)/shard_map/all_to_all | solution.py:19
  181.3 7.7 %all-to-all-done.4 = f32[32,1,128]{2,1,0:T(1,128)S(1)} async-done(((f32[32,1,128]{2,1,0:T(1,128)}), f32[32,1,128]{2,1,0:T(1,128)S(1)}, u32[]{:S(2)}, u32[]{:S(2)}) %all-to-all-start.4) | async-done | bytes 16416 | tf_op jit(solution)/shard_map/all_to_all | solution.py:19
  (40 shorter events, 4.3 us)
Async XLA Ops:
  8.8 77.5 %all-to-all-start = ((bf16[32,64,128]{2,1,0:T(8,128)(2,1)}), bf16[32,64,128]{2,1,0:T(8,128)(2,1)S(1)}, u32[]{:S(2)}, u32[]{:S(2)}) async-start(bf16[32,64,128]{2,1,0:T(8,128)(2,1)} %broadcast_in_dim.10), calls=%async_computation | async-start | bytes 1048576 | tf_op jit(solution)/shard_map/all_to_all | solution.py:19
  25.5 99.0 %all-gather.2.cloned.1.call-start = ((), (), s32[]{:S(2)}) async-start(), calls=%async_computation.5 | async-start | bytes 1183744 | tf_op jit(solution)/shard_map/all_gather | solution.py:206
  66.4 20.0 %copy-start = (bf16[2176,128]{1,0:T(8,128)(2,1)}, bf16[2176,128]{1,0:T(8,128)(2,1)S(1)}, u32[]{:S(2)}) copy-start(bf16[2176,128]{1,0:T(8,128)(2,1)S(1)} %all_gather.6.refs_0_) | copy-start | bytes 1671172
  66.4 12.0 %collective-permute-start.1 = (bf16[1088,128]{1,0:T(8,128)(2,1)S(1)}, bf16[1088,128]{1,0:T(8,128)(2,1)S(1)}, u32[]{:S(2)}, u32[]{:S(2)}) collective-permute-start(bf16[1088,128]{1,0:T(8,128)(2,1)S(1)} %get-tuple-element.26), channel_id=1, source_target_pairs={{0,960},{64,0},{128,64},{192,128},{256,192},{320,256},{384,320},{4... | collective-permute-start | bytes 835592 | tf_op jit(solution)/shard_map/ppermute | solution.py:65
  72.1 10.8 %collective-permute-start.2 = (bf16[1088,128]{1,0:T(8,128)(2,1)S(1)}, bf16[1088,128]{1,0:T(8,128)(2,1)S(1)}, u32[]{:S(2)}, u32[]{:S(2)}) collective-permute-start(bf16[1088,128]{1,0:T(8,128)(2,1)S(1)} %get-tuple-element.25), channel_id=1, source_target_pairs={{0,64},{64,128},{128,192},{192,256},{256,320},{320,384},{384,448},... | collective-permute-start | bytes 835592 | tf_op jit(solution)/shard_map/ppermute | solution.py:66
  74.0 12.3 %collective-permute-start = (bf16[2176,128]{1,0:T(8,128)(2,1)S(1)}, bf16[2176,128]{1,0:T(8,128)(2,1)S(1)}, u32[]{:S(2)}, u32[]{:S(2)}) collective-permute-start(bf16[2176,128]{1,0:T(8,128)(2,1)S(1)} %all_gather.6.refs_0_), channel_id=1, source_target_pairs={{0,32},{32,0},{1,33},{33,1},{2,34},{34,2},{3,35},{35,3},{4,36},{36... | collective-permute-start | bytes 1671176 | tf_op jit(solution)/shard_map/ppermute | solution.py:71
  78.4 7.9 %copy-start.6 = (bf16[1088,128]{1,0:T(8,128)(2,1)}, bf16[1088,128]{1,0:T(8,128)(2,1)S(1)}, u32[]{:S(2)}) copy-start(bf16[1088,128]{1,0:T(8,128)(2,1)S(1)} %collective-permute-done.1.refs_2_) | copy-start | bytes 835588
  78.4 6.9 %collective-permute-start.3 = (bf16[1088,128]{1,0:T(8,128)(2,1)S(1)}, bf16[1088,128]{1,0:T(8,128)(2,1)S(1)}, u32[]{:S(2)}, u32[]{:S(2)}) collective-permute-start(bf16[1088,128]{1,0:T(8,128)(2,1)S(1)} %collective-permute-done.1.refs_2_), channel_id=1, source_target_pairs={{0,32},{32,0},{1,33},{33,1},{2,34},{34,2},{3,35},{35,3},{4,36},{36... | collective-permute-start | bytes 835592 | tf_op jit(solution)/shard_map/ppermute | solution.py:71
  82.9 3.5 %copy-start.7 = (bf16[1088,128]{1,0:T(8,128)(2,1)}, bf16[1088,128]{1,0:T(8,128)(2,1)S(1)}, u32[]{:S(2)}) copy-start(bf16[1088,128]{1,0:T(8,128)(2,1)S(1)} %collective-permute-done.2.refs_3_) | copy-start | bytes 835588
  82.9 3.4 %collective-permute-start.4 = (bf16[1088,128]{1,0:T(8,128)(2,1)S(1)}, bf16[1088,128]{1,0:T(8,128)(2,1)S(1)}, u32[]{:S(2)}, u32[]{:S(2)}) collective-permute-start(bf16[1088,128]{1,0:T(8,128)(2,1)S(1)} %collective-permute-done.2.refs_3_), channel_id=1, source_target_pairs={{0,32},{32,0},{1,33},{33,1},{2,34},{34,2},{3,35},{35,3},{4,36},{36... | collective-permute-start | bytes 835592 | tf_op jit(solution)/shard_map/ppermute | solution.py:71
  85.4 1.0 copy-start.8
  86.3 0.7 copy-start.9
  86.3 0.9 copy-start.3
  86.3 1.1 copy-start.1
  118.9 21.5 %all-to-all-start.2 = ((bf16[32,64,128]{2,1,0:T(8,128)(2,1)}), bf16[32,64,128]{2,1,0:T(8,128)(2,1)S(1)}, u32[]{:S(2)}, u32[]{:S(2)}) async-start(bf16[32,64,128]{2,1,0:T(8,128)(2,1)} %broadcast_in_dim.12), calls=%async_computation.2 | async-start | bytes 1048576 | tf_op jit(solution)/shard_map/all_to_all | solution.py:19
  124.4 16.3 %copy-start.2 = (bf16[32,64,128]{2,1,0:T(8,128)(2,1)S(1)}, bf16[32,64,128]{2,1,0:T(8,128)(2,1)}, u32[]{:S(2)}) copy-start(bf16[32,64,128]{2,1,0:T(8,128)(2,1)} %copy-done.1) | copy-start | bytes 1572868
  124.4 16.3 %copy-start.10 = (f32[2048]{0:T(1024)S(1)}, f32[2048]{0:T(1024)}, u32[]{:S(2)}) copy-start(f32[2048]{0:T(1024)} %param.16) | copy-start | bytes 24580
  125.8 16.0 %collective-permute-start.5 = (bf16[2176,128]{1,0:T(8,128)(2,1)S(1)}, bf16[2176,128]{1,0:T(8,128)(2,1)S(1)}, u32[]{:S(2)}, u32[]{:S(2)}) collective-permute-start(bf16[2176,128]{1,0:T(8,128)(2,1)S(1)} %get-tuple-element.24), channel_id=1, source_target_pairs={{0,960},{64,0},{128,64},{192,128},{256,192},{320,256},{384,320},{4... | collective-permute-start | bytes 1671176 | tf_op jit(solution)/shard_map/ppermute | solution.py:65
  129.4 16.0 %collective-permute-start.6 = (bf16[2176,128]{1,0:T(8,128)(2,1)S(1)}, bf16[2176,128]{1,0:T(8,128)(2,1)S(1)}, u32[]{:S(2)}, u32[]{:S(2)}) collective-permute-start(bf16[2176,128]{1,0:T(8,128)(2,1)S(1)} %get-tuple-element.23), channel_id=1, source_target_pairs={{0,64},{64,128},{128,192},{192,256},{256,320},{320,384},{384,448},... | collective-permute-start | bytes 1671176 | tf_op jit(solution)/shard_map/ppermute | solution.py:66
  141.9 3.5 %copy-start.4 = (bf16[2176,128]{1,0:T(8,128)(2,1)}, bf16[2176,128]{1,0:T(8,128)(2,1)S(1)}, u32[]{:S(2)}) copy-start(bf16[2176,128]{1,0:T(8,128)(2,1)S(1)} %collective-permute-done.5.refs_1_) | copy-start | bytes 1671172
  145.4 0.8 copy-start.5
  149.9 24.3 %all-to-all-start.3 = ((bf16[32,64,128]{2,1,0:T(8,128)(2,1)}), bf16[32,64,128]{2,1,0:T(8,128)(2,1)S(1)}, u32[]{:S(2)}, u32[]{:S(2)}) async-start(bf16[32,64,128]{2,1,0:T(8,128)(2,1)} %bitcast.27), calls=%async_computation.3 | async-start | bytes 1048576 | tf_op jit(solution)/shard_map/all_to_all | solution.py:28
  175.0 14.0 %all-to-all-start.4 = ((f32[32,1,128]{2,1,0:T(1,128)}), f32[32,1,128]{2,1,0:T(1,128)S(1)}, u32[]{:S(2)}, u32[]{:S(2)}) async-start(f32[32,1,128]{2,1,0:T(1,128)} %broadcast_in_dim.14), calls=%async_computation.4 | async-start | bytes 32768 | tf_op jit(solution)/shard_map/all_to_all | solution.py:19
Sparse Core Ops, SparseCore 0:
  29.6 55.7 all-gather.1

commit v3 on v2

--- a/solution.py
+++ b/solution.py
@@ -40,23 +40,27 @@
     return aligned(-(-3 * aligned(hidden) // 2))
 
 
-def packed(gain, gate, up, down):
-    rows, hidden = gate.shape
+def packed(*groups):
+    rows, hidden = groups[0][1].shape
     block, half = aligned(hidden), packed_rows(hidden)
-
-    def kernel(gain_ref, gate_ref, up_ref, down_ref, out_ref, tall_ref):
+    count = len(groups)
+
+    def kernel(*refs):
+        outs, tall_ref = refs[4 * count : -1], refs[-1]
         tall_ref[...] = jnp.zeros_like(tall_ref)
-        tall_ref[:hidden, :] = gate_ref[...].T * gain_ref[...]
-        tall_ref[block : block + hidden, :] = up_ref[...].T * gain_ref[...]
-        tall_ref[2 * block : 2 * block + hidden, :] = down_ref[...].T
-        halves = (tall_ref[:half, :], tall_ref[half:, :])
-        out_ref[...] = jnp.concatenate(halves, axis=1).astype(jnp.bfloat16)
+        for i, out_ref in enumerate(outs):
+            gain_ref, gate_ref, up_ref, down_ref = refs[4 * i : 4 * i + 4]
+            tall_ref[i, :hidden, :] = gate_ref[...].T * gain_ref[...]
+            tall_ref[i, block : block + hidden, :] = up_ref[...].T * gain_ref[...]
+            tall_ref[i, 2 * block : 2 * block + hidden, :] = down_ref[...].T
+            halves = (tall_ref[i, :half, :], tall_ref[i, half:, :])
+            out_ref[...] = jnp.concatenate(halves, axis=1).astype(jnp.bfloat16)
 
     return pl.pallas_call(
         kernel,
-        out_shape=jax.ShapeDtypeStruct((half, 2 * rows), jnp.bfloat16),
-        scratch_shapes=[pltpu.VMEM((2 * half, rows), jnp.float32)],
-    )(gain[None, :], gate, up, down.T)
+        out_shape=[jax.ShapeDtypeStruct((half, 2 * rows), jnp.bfloat16)] * count,
+        scratch_shapes=[pltpu.VMEM((count, 2 * half, rows), jnp.float32)],
+    )(*(a for gain, gate, up, down in groups for a in (gain[None, :], gate, up, down.T)))
 
 
 def from_neighbours(own):
@@ -201,8 +205,10 @@
     column_start = lax.axis_index(TP) * columns
     full = gathered_copies(tokens.T, TP)
     place = jnp.stack([lax.axis_index("parity"), lax.axis_index("core")]).astype(jnp.int32)
-    rows_one = packed(first_gain, first_gate, first_up, first_down)
-    rows_two = packed(second_gain, second_gate, second_up, second_down)
+    rows_one, rows_two = packed(
+        (first_gain, first_gate, first_up, first_down),
+        (second_gain, second_gate, second_up, second_down),
+    )
     own_two = lax.all_gather(rows_two, ("pair", "core"), axis=0, tiled=True)
     own_one = lax.all_gather(rows_one, "pair", axis=0, tiled=True)
     near_one = from_neighbours(own_one)

time: 198 us -> 197 us (level)
  no operation moved by 1% of the time
where the time goes in v3:
time: 197 us; the launch traced here: 196 us
  blocking collectives  63.8 us (32%)
  starting transfers between devices  57.1 us (29%)
  waiting for transfers between devices  33 us (17%)
  Pallas kernels  16.9 us (9%)
  between operations  14.2 us (7%)
  local copies, waits for them, and re-layouts  6.37 us (3%)
  other arithmetic  4.49 us (2%)
    all_gather x1, blocking collectives, on_device(): own_one = lax.all_gather(rows_one, 'pair', axis=0, tiled=True)  36.6 us
    all_to_all x3, starting transfers between devices, sent_to_all(): lax.all_to_all(jnp.broadcast_to(x[None], (peers, *x.shape)), axis, 0, 0,...  27.8 us
    all_to_all x1, blocking collectives, sent_and_summed(): lax.all_to_all(x.reshape(peers, -1, *x.shape[1:]), axis, 0, 0, tiled=True)  27.2 us
    all_to_all x3, waiting for transfers between devices, sent_to_all(): lax.all_to_all(jnp.broadcast_to(x[None], (peers, *x.shape)), axis, 0, 0,...  16.5 us
    ppermute x2, starting transfers between devices, from_neighbours(): lax.ppermute(own[:half], FS[:2], [(i, (i - 1) % ring) for i in range(ring)])  9.9 us
    all_to_all x1, starting transfers between devices, sent_and_summed(): lax.all_to_all(x.reshape(peers, -1, *x.shape[1:]), axis, 0, 0, tiled=True)  9.77 us
    pallas_call x2, Pallas kernels, mixed_part(): pl.pallas_call(kernel, in_specs=[pl.BlockSpec(memory_space=pltpu.SMEM)] +...  7.58 us
    pallas_call x2, Pallas kernels, sampler_slabs(): pl.pallas_call(kernel, in_specs=[pl.BlockSpec(memory_space=pltpu.SMEM)] +...  7.29 us
  transfers between devices with their start and end apart: 12, of which 7 were waited for; matrix products, arithmetic and copies ran while one was open for 3% of the time, Pallas kernels for 7%

profile of v3, /device:TPU:2, one launch (start us, length us, event | category | flops | bytes accessed | tf_op | source)
XLA Modules:
  0.0 195.8 jit_solution(6493304388197401490)
XLA Ops:
  7.2 1.6 broadcast_in_dim.10
  8.8 16.7 %all-to-all-start = ((bf16[32,64,128]{2,1,0:T(8,128)(2,1)}), bf16[32,64,128]{2,1,0:T(8,128)(2,1)S(1)}, u32[]{:S(2)}, u32[]{:S(2)}) async-start(bf16[32,64,128]{2,1,0:T(8,128)(2,1)} %broadcast_in_dim.10), calls=%async_computation | async-start | bytes 1048576 | tf_op jit(solution)/shard_map/all_to_all | solution.py:19
  25.6 2.0 %shard_map.162 = (bf16[272,128]{1,0:T(8,128)(2,1)}, bf16[272,128]{1,0:T(8,128)(2,1)}) custom-call(f32[1,64]{1,0:T(1,128)} %bitcast.33, f32[64,172]{1,0:T(8,128)} %refs_1_.1, f32[64,172]{1,0:T(8,128)} %refs_2_.1, f32[64,172]{1,0:T(8,128)} %bitcast.30, f32[1,64]{1,0:T(1,128)} %bitcast.34, f32[64,172]{1,0:T(8,128)} %refs_5_.1, f32[64,172]{1,0:T(8,128)} %refs_6_.1, ...), custom_call_target="tpu_custom_call" | custom-call | tf_op jit(solution)/shard_map/pallas_call | solution.py:59
  27.6 36.6 %all_gather.6.refs_0_ = bf16[2176,128]{1,0:T(8,128)(2,1)S(1)} all-gather(bf16[272,128]{1,0:T(8,128)(2,1)} %get-tuple-element.17), channel_id=1, replica_groups=mesh['pair'=8,'parity'=2,'core'=2,'tp_0'=8,'tp_1'=4] {'pair'}, dimensions={0}, use_global_device_ids=true | all-gather | bytes 626688 | tf_op jit(solution)/shard_map/all_gather | solution.py:213
  64.3 6.0 %collective-permute-start.1 = (bf16[1088,128]{1,0:T(8,128)(2,1)S(1)}, bf16[1088,128]{1,0:T(8,128)(2,1)S(1)}, u32[]{:S(2)}, u32[]{:S(2)}) collective-permute-start(bf16[1088,128]{1,0:T(8,128)(2,1)S(1)} %get-tuple-element.30), channel_id=1, source_target_pairs={{0,960},{64,0},{128,64},{192,128},{256,192},{320,256},{384,320},{4... | collective-permute-start | bytes 835592 | tf_op jit(solution)/shard_map/ppermute | solution.py:69
  70.2 1.9 collective-permute-start.2
  72.2 1.9 collective-permute-start
  74.1 2.0 %collective-permute-done.1.refs_2_ = bf16[1088,128]{1,0:T(8,128)(2,1)S(1)} collective-permute-done((bf16[1088,128]{1,0:T(8,128)(2,1)S(1)}, bf16[1088,128]{1,0:T(8,128)(2,1)S(1)}, u32[]{:S(2)}, u32[]{:S(2)}) %collective-permute-start.1) | collective-permute-done | bytes 278560 | tf_op jit(solution)/shard_map/ppermute | solution.py:69
  76.1 1.9 collective-permute-start.3
  78.0 3.3 %collective-permute-done.2.refs_3_ = bf16[1088,128]{1,0:T(8,128)(2,1)S(1)} collective-permute-done((bf16[1088,128]{1,0:T(8,128)(2,1)S(1)}, bf16[1088,128]{1,0:T(8,128)(2,1)S(1)}, u32[]{:S(2)}, u32[]{:S(2)}) %collective-permute-start.2) | collective-permute-done | bytes 278560 | tf_op jit(solution)/shard_map/ppermute | solution.py:70
  81.3 1.9 collective-permute-start.4
  83.9 0.9 collective-permute-done.4.refs_5_
  85.8 3.8 %shard_map.163 = bf16[2048,128]{1,0:T(8,128)(2,1)} custom-call(s32[2]{0:T(128)} %pad_add_fusion.place_ref, bf16[2176,128]{1,0:T(8,128)(2,1)} %copy-done, bf16[2176,128]{1,0:T(8,128)(2,1)} %copy-done.3, bf16[1088,128]{1,0:T(8,128)(2,1)} %copy-done.6, bf16[1088,128]{1,0:T(8,128)(2,1)} %copy-done.7, bf16[1088,128]{1,0:T(8,128)(2,1)} %copy-done.8, ...), custom_call_target="tpu_custom_call" | custom-call | tf_op jit(solution)/shard_map/pallas_call | solution.py:151
  89.6 27.2 %all_to_all.25 = bf16[32,64,128]{2,1,0:T(8,128)(2,1)S(1)} all-to-all(bf16[32,64,128]{2,1,0:T(8,128)(2,1)} %bitcast.28), channel_id=1, replica_groups=mesh['pair'=8,'parity'=2,'core'=2,'tp_0'=8,'tp_1'=4] {'tp_0','tp_1'}, dimensions={0} | all-to-all | bytes 1048576 | tf_op jit(solution)/shard_map/all_to_all | solution.py:28
  116.8 0.9 broadcast_in_dim.13
  117.7 5.6 %all-to-all-start.2 = ((bf16[32,64,128]{2,1,0:T(8,128)(2,1)}), bf16[32,64,128]{2,1,0:T(8,128)(2,1)S(1)}, u32[]{:S(2)}, u32[]{:S(2)}) async-start(bf16[32,64,128]{2,1,0:T(8,128)(2,1)} %broadcast_in_dim.13), calls=%async_computation.2 | async-start | bytes 1048576 | tf_op jit(solution)/shard_map/all_to_all | solution.py:19
  123.4 1.3 fusion.4
  124.7 3.9 %collective-permute-start.5 = (bf16[2176,128]{1,0:T(8,128)(2,1)S(1)}, bf16[2176,128]{1,0:T(8,128)(2,1)S(1)}, u32[]{:S(2)}, u32[]{:S(2)}) collective-permute-start(bf16[2176,128]{1,0:T(8,128)(2,1)S(1)} %get-tuple-element.28), channel_id=1, source_target_pairs={{0,960},{64,0},{128,64},{192,128},{256,192},{320,256},{384,320},{4... | collective-permute-start | bytes 1671176 | tf_op jit(solution)/shard_map/ppermute | solution.py:69
  128.7 1.9 collective-permute-start.6
  130.6 8.7 %all-to-all-done.2 = bf16[32,64,128]{2,1,0:T(8,128)(2,1)S(1)} async-done(((bf16[32,64,128]{2,1,0:T(8,128)(2,1)}), bf16[32,64,128]{2,1,0:T(8,128)(2,1)S(1)}, u32[]{:S(2)}, u32[]{:S(2)}) %all-to-all-start.2) | async-done | bytes 524320 | tf_op jit(solution)/shard_map/all_to_all | solution.py:19
  139.6 1.1 fusion.2.refs_3_
  140.8 3.9 %collective-permute-done.6.refs_2_ = bf16[2176,128]{1,0:T(8,128)(2,1)S(1)} collective-permute-done((bf16[2176,128]{1,0:T(8,128)(2,1)S(1)}, bf16[2176,128]{1,0:T(8,128)(2,1)S(1)}, u32[]{:S(2)}, u32[]{:S(2)}) %collective-permute-start.6) | collective-permute-done | bytes 557088 | tf_op jit(solution)/shard_map/ppermute | solution.py:70
  144.6 0.8 copy-done.5
  145.4 3.8 %shard_map.164 = bf16[2048,128]{1,0:T(8,128)(2,1)} custom-call(s32[2]{0:T(128)} %pad_add_fusion.place_ref, bf16[4352,128]{1,0:T(8,128)(2,1)} %all-gather.2.cloned.1.call-done.refs_0_, bf16[2176,128]{1,0:T(8,128)(2,1)} %copy-done.4, bf16[2176,128]{1,0:T(8,128)(2,1)} %copy-done.5, bf16[2048,128]{1,0:T(8,128)(2,1)} %fusion.2.refs_3_), custom_call_target="tpu_custom_call" | custom-call | tf_op jit(solution)/shard_map/pallas_call | solution.py:151
  149.2 9.8 %all-to-all-start.3 = ((bf16[32,64,128]{2,1,0:T(8,128)(2,1)}), bf16[32,64,128]{2,1,0:T(8,128)(2,1)S(1)}, u32[]{:S(2)}, u32[]{:S(2)}) async-start(bf16[32,64,128]{2,1,0:T(8,128)(2,1)} %bitcast.27), calls=%async_computation.3 | async-start | bytes 1048576 | tf_op jit(solution)/shard_map/all_to_all | solution.py:28
  159.0 0.8 dynamic-slice_multiply_fusion
  159.8 3.7 %shard_map.165 = (bf16[172,2048]{1,0:T(8,128)(2,1)}, bf16[172,2048]{1,0:T(8,128)(2,1)}, bf16[172,2048]{1,0:T(8,128)(2,1)}) custom-call(s32[2]{0:T(128)} %pad_add_fusion.place_ref, bf16[2176,128]{1,0:T(8,128)(2,1)} %copy-done, bf16[2176,128]{1,0:T(8,128)(2,1)} %copy-done.3, bf16[1088,128]{1,0:T(8,128)(2,1)} %copy-done.6, bf16[1088,128]{1,0:T(8,128)(2,1)} %copy-done.7, ...), custom_call_target="tpu_custom_call" | custom-call | tf_op jit(solution)/shard_map/pallas_call | solution.py:182
  163.5 3.6 %shard_map.166 = (bf16[172,2048]{1,0:T(8,128)(2,1)}, bf16[172,2048]{1,0:T(8,128)(2,1)}, bf16[172,2048]{1,0:T(8,128)(2,1)}) custom-call(s32[2]{0:T(128)} %pad_add_fusion.place_ref, bf16[4352,128]{1,0:T(8,128)(2,1)} %all-gather.2.cloned.1.call-done.refs_0_, bf16[2176,128]{1,0:T(8,128)(2,1)} %copy-done.4, bf16[2176,128]{1,0:T(8,128)(2,1)} %copy-done.5), custom_call_target="tpu_custom_call" | custom-call | tf_op jit(solution)/shard_map/pallas_call | solution.py:182
  167.1 6.4 %all-to-all-done.3 = bf16[32,64,128]{2,1,0:T(8,128)(2,1)S(1)} async-done(((bf16[32,64,128]{2,1,0:T(8,128)(2,1)}), bf16[32,64,128]{2,1,0:T(8,128)(2,1)S(1)}, u32[]{:S(2)}, u32[]{:S(2)}) %all-to-all-start.3) | async-done | bytes 524320 | tf_op jit(solution)/shard_map/all_to_all | solution.py:28
  174.3 5.6 %all-to-all-start.4 = ((f32[32,1,128]{2,1,0:T(1,128)}), f32[32,1,128]{2,1,0:T(1,128)S(1)}, u32[]{:S(2)}, u32[]{:S(2)}) async-start(f32[32,1,128]{2,1,0:T(1,128)} %broadcast_in_dim.14), calls=%async_computation.4 | async-start | bytes 32768 | tf_op jit(solution)/shard_map/all_to_all | solution.py:19
  179.9 0.7 dynamic-slice_convert_fusion
  180.6 7.7 %all-to-all-done.4 = f32[32,1,128]{2,1,0:T(1,128)S(1)} async-done(((f32[32,1,128]{2,1,0:T(1,128)}), f32[32,1,128]{2,1,0:T(1,128)S(1)}, u32[]{:S(2)}, u32[]{:S(2)}) %all-to-all-start.4) | async-done | bytes 16416 | tf_op jit(solution)/shard_map/all_to_all | solution.py:19
  (39 shorter events, 3.6 us)
Async XLA Ops:
  8.8 76.0 %all-to-all-start = ((bf16[32,64,128]{2,1,0:T(8,128)(2,1)}), bf16[32,64,128]{2,1,0:T(8,128)(2,1)S(1)}, u32[]{:S(2)}, u32[]{:S(2)}) async-start(bf16[32,64,128]{2,1,0:T(8,128)(2,1)} %broadcast_in_dim.10), calls=%async_computation | async-start | bytes 1048576 | tf_op jit(solution)/shard_map/all_to_all | solution.py:19
  25.5 97.9 %all-gather.2.cloned.1.call-start = ((), (), s32[]{:S(2)}) async-start(), calls=%async_computation.5 | async-start | bytes 1183744 | tf_op jit(solution)/shard_map/all_gather | solution.py:212
  64.2 20.6 %copy-start = (bf16[2176,128]{1,0:T(8,128)(2,1)}, bf16[2176,128]{1,0:T(8,128)(2,1)S(1)}, u32[]{:S(2)}) copy-start(bf16[2176,128]{1,0:T(8,128)(2,1)S(1)} %all_gather.6.refs_0_) | copy-start | bytes 1671172
  64.3 11.8 %collective-permute-start.1 = (bf16[1088,128]{1,0:T(8,128)(2,1)S(1)}, bf16[1088,128]{1,0:T(8,128)(2,1)S(1)}, u32[]{:S(2)}, u32[]{:S(2)}) collective-permute-start(bf16[1088,128]{1,0:T(8,128)(2,1)S(1)} %get-tuple-element.30), channel_id=1, source_target_pairs={{0,960},{64,0},{128,64},{192,128},{256,192},{320,256},{384,320},{4... | collective-permute-start | bytes 835592 | tf_op jit(solution)/shard_map/ppermute | solution.py:69
  70.2 11.1 %collective-permute-start.2 = (bf16[1088,128]{1,0:T(8,128)(2,1)S(1)}, bf16[1088,128]{1,0:T(8,128)(2,1)S(1)}, u32[]{:S(2)}, u32[]{:S(2)}) collective-permute-start(bf16[1088,128]{1,0:T(8,128)(2,1)S(1)} %get-tuple-element.29), channel_id=1, source_target_pairs={{0,64},{64,128},{128,192},{192,256},{256,320},{320,384},{384,448},... | collective-permute-start | bytes 835592 | tf_op jit(solution)/shard_map/ppermute | solution.py:70
  72.2 12.6 %collective-permute-start = (bf16[2176,128]{1,0:T(8,128)(2,1)S(1)}, bf16[2176,128]{1,0:T(8,128)(2,1)S(1)}, u32[]{:S(2)}, u32[]{:S(2)}) collective-permute-start(bf16[2176,128]{1,0:T(8,128)(2,1)S(1)} %all_gather.6.refs_0_), channel_id=1, source_target_pairs={{0,32},{32,0},{1,33},{33,1},{2,34},{34,2},{3,35},{35,3},{4,36},{36... | collective-permute-start | bytes 1671176 | tf_op jit(solution)/shard_map/ppermute | solution.py:75
  76.1 8.7 %copy-start.6 = (bf16[1088,128]{1,0:T(8,128)(2,1)}, bf16[1088,128]{1,0:T(8,128)(2,1)S(1)}, u32[]{:S(2)}) copy-start(bf16[1088,128]{1,0:T(8,128)(2,1)S(1)} %collective-permute-done.1.refs_2_) | copy-start | bytes 835588
  76.1 7.8 %collective-permute-start.3 = (bf16[1088,128]{1,0:T(8,128)(2,1)S(1)}, bf16[1088,128]{1,0:T(8,128)(2,1)S(1)}, u32[]{:S(2)}, u32[]{:S(2)}) collective-permute-start(bf16[1088,128]{1,0:T(8,128)(2,1)S(1)} %collective-permute-done.1.refs_2_), channel_id=1, source_target_pairs={{0,32},{32,0},{1,33},{33,1},{2,34},{34,2},{3,35},{35,3},{4,36},{36... | collective-permute-start | bytes 835592 | tf_op jit(solution)/shard_map/ppermute | solution.py:75
  81.3 3.5 %copy-start.7 = (bf16[1088,128]{1,0:T(8,128)(2,1)}, bf16[1088,128]{1,0:T(8,128)(2,1)S(1)}, u32[]{:S(2)}) copy-start(bf16[1088,128]{1,0:T(8,128)(2,1)S(1)} %collective-permute-done.2.refs_3_) | copy-start | bytes 835588
  81.3 3.4 %collective-permute-start.4 = (bf16[1088,128]{1,0:T(8,128)(2,1)S(1)}, bf16[1088,128]{1,0:T(8,128)(2,1)S(1)}, u32[]{:S(2)}, u32[]{:S(2)}) collective-permute-start(bf16[1088,128]{1,0:T(8,128)(2,1)S(1)} %collective-permute-done.2.refs_3_), channel_id=1, source_target_pairs={{0,32},{32,0},{1,33},{33,1},{2,34},{34,2},{3,35},{35,3},{4,36},{36... | collective-permute-start | bytes 835592 | tf_op jit(solution)/shard_map/ppermute | solution.py:75
  83.9 0.9 copy-start.8
  84.7 0.7 copy-start.9
  84.7 0.9 copy-start.3
  84.8 1.1 copy-start.1
  117.7 21.6 %all-to-all-start.2 = ((bf16[32,64,128]{2,1,0:T(8,128)(2,1)}), bf16[32,64,128]{2,1,0:T(8,128)(2,1)S(1)}, u32[]{:S(2)}, u32[]{:S(2)}) async-start(bf16[32,64,128]{2,1,0:T(8,128)(2,1)} %broadcast_in_dim.13), calls=%async_computation.2 | async-start | bytes 1048576 | tf_op jit(solution)/shard_map/all_to_all | solution.py:19
  123.3 16.3 %copy-start.2 = (bf16[32,64,128]{2,1,0:T(8,128)(2,1)S(1)}, bf16[32,64,128]{2,1,0:T(8,128)(2,1)}, u32[]{:S(2)}) copy-start(bf16[32,64,128]{2,1,0:T(8,128)(2,1)} %copy-done.1) | copy-start | bytes 1572868
  123.3 16.3 %copy-start.10 = (f32[2048]{0:T(1024)S(1)}, f32[2048]{0:T(1024)}, u32[]{:S(2)}) copy-start(f32[2048]{0:T(1024)} %param.16) | copy-start | bytes 24580
  124.7 16.0 %collective-permute-start.5 = (bf16[2176,128]{1,0:T(8,128)(2,1)S(1)}, bf16[2176,128]{1,0:T(8,128)(2,1)S(1)}, u32[]{:S(2)}, u32[]{:S(2)}) collective-permute-start(bf16[2176,128]{1,0:T(8,128)(2,1)S(1)} %get-tuple-element.28), channel_id=1, source_target_pairs={{0,960},{64,0},{128,64},{192,128},{256,192},{320,256},{384,320},{4... | collective-permute-start | bytes 1671176 | tf_op jit(solution)/shard_map/ppermute | solution.py:69
  128.7 16.0 %collective-permute-start.6 = (bf16[2176,128]{1,0:T(8,128)(2,1)S(1)}, bf16[2176,128]{1,0:T(8,128)(2,1)S(1)}, u32[]{:S(2)}, u32[]{:S(2)}) collective-permute-start(bf16[2176,128]{1,0:T(8,128)(2,1)S(1)} %get-tuple-element.27), channel_id=1, source_target_pairs={{0,64},{64,128},{128,192},{192,256},{256,320},{320,384},{384,448},... | collective-permute-start | bytes 1671176 | tf_op jit(solution)/shard_map/ppermute | solution.py:70
  140.8 3.9 %copy-start.4 = (bf16[2176,128]{1,0:T(8,128)(2,1)}, bf16[2176,128]{1,0:T(8,128)(2,1)S(1)}, u32[]{:S(2)}) copy-start(bf16[2176,128]{1,0:T(8,128)(2,1)S(1)} %collective-permute-done.5.refs_1_) | copy-start | bytes 1671172
  144.6 0.8 copy-start.5
  149.2 24.3 %all-to-all-start.3 = ((bf16[32,64,128]{2,1,0:T(8,128)(2,1)}), bf16[32,64,128]{2,1,0:T(8,128)(2,1)S(1)}, u32[]{:S(2)}, u32[]{:S(2)}) async-start(bf16[32,64,128]{2,1,0:T(8,128)(2,1)} %bitcast.27), calls=%async_computation.3 | async-start | bytes 1048576 | tf_op jit(solution)/shard_map/all_to_all | solution.py:28
  174.3 14.1 %all-to-all-start.4 = ((f32[32,1,128]{2,1,0:T(1,128)}), f32[32,1,128]{2,1,0:T(1,128)S(1)}, u32[]{:S(2)}, u32[]{:S(2)}) async-start(f32[32,1,128]{2,1,0:T(1,128)} %broadcast_in_dim.14), calls=%async_computation.4 | async-start | bytes 32768 | tf_op jit(solution)/shard_map/all_to_all | solution.py:19
Sparse Core Ops, SparseCore 0:
  29.6 55.5 all-gather.1

commit v4 on v3

--- a/solution.py
+++ b/solution.py
@@ -63,11 +63,16 @@
     )(*(a for gain, gate, up, down in groups for a in (gain[None, :], gate, up, down.T)))
 
 
-def from_neighbours(own):
+def first_share(pairs, alone):
+    return pairs * 5 // 8 if alone else pairs // 2
+
+
+def from_neighbours(own, alone):
     ring = lax.axis_size(FS[:2])
-    half = own.shape[0] // 2
-    low = lax.ppermute(own[:half], FS[:2], [(i, (i - 1) % ring) for i in range(ring)])
-    high = lax.ppermute(own[half:], FS[:2], [(i, (i + 1) % ring) for i in range(ring)])
+    pairs = ring // 2
+    cut = own.shape[0] // pairs * first_share(pairs, alone)
+    low = lax.ppermute(own[:cut], FS[:2], [(i, (i - 1) % ring) for i in range(ring)])
+    high = lax.ppermute(own[cut:], FS[:2], [(i, (i + 1) % ring) for i in range(ring)])
     return low, high
 
 
@@ -80,8 +85,9 @@
     alone = len(refs) == 6
     pairs = refs[0].shape[0] // half // (1 if alone else 2)
     for at in range(pairs):
-        late = at >= pairs // 2
-        row = at % (pairs // 2)
+        share = first_share(pairs, alone)
+        late = at >= share
+        row = at - share if late else at
         if alone:
             own, mate, low, high, mate_low, mate_high = refs
             sides = (
@@ -211,10 +217,10 @@
     )
     own_two = lax.all_gather(rows_two, ("pair", "core"), axis=0, tiled=True)
     own_one = lax.all_gather(rows_one, "pair", axis=0, tiled=True)
-    near_one = from_neighbours(own_one)
+    near_one = from_neighbours(own_one, True)
     mates_one = [from_partner(x) for x in (own_one, *near_one)]
     slabs_one = (own_one, mates_one[0], *near_one, *mates_one[1:])
-    slabs_two = (own_two, *from_neighbours(own_two))
+    slabs_two = (own_two, *from_neighbours(own_two, False))
     features = full.shape[0]
     gate_one, up_one, down_one = sampler_slabs(place, slabs_one, hidden, features)
     gate_two, up_two, down_two = sampler_slabs(place, slabs_two, hidden, features)

time: 197 us -> 196 us (level)
  no operation moved by 1% of the time
where the time goes in v4:
time: 196 us; the launch traced here: 195 us
  blocking collectives  62.8 us (32%)
  starting transfers between devices  57.2 us (29%)
  waiting for transfers between devices  32.6 us (17%)
  Pallas kernels  16.9 us (9%)
  between operations  14.2 us (7%)
  local copies, waits for them, and re-layouts  6.46 us (3%)
  other arithmetic  4.47 us (2%)
    all_gather x1, blocking collectives, on_device(): own_one = lax.all_gather(rows_one, 'pair', axis=0, tiled=True)  36.1 us
    all_to_all x3, starting transfers between devices, sent_to_all(): lax.all_to_all(jnp.broadcast_to(x[None], (peers, *x.shape)), axis, 0, 0,...  27.8 us
    all_to_all x1, blocking collectives, sent_and_summed(): lax.all_to_all(x.reshape(peers, -1, *x.shape[1:]), axis, 0, 0, tiled=True)  26.7 us
    all_to_all x3, waiting for transfers between devices, sent_to_all(): lax.all_to_all(jnp.broadcast_to(x[None], (peers, *x.shape)), axis, 0, 0,...  16.5 us
    all_to_all x1, starting transfers between devices, sent_and_summed(): lax.all_to_all(x.reshape(peers, -1, *x.shape[1:]), axis, 0, 0, tiled=True)  9.77 us
    ppermute x2, starting transfers between devices, from_neighbours(): lax.ppermute(own[:cut], FS[:2], [(i, (i - 1) % ring) for i in range(ring)])  7.94 us
    ppermute x2, waiting for transfers between devices, from_neighbours(): lax.ppermute(own[cut:], FS[:2], [(i, (i + 1) % ring) for i in range(ring)])  7.89 us
    pallas_call x2, Pallas kernels, mixed_part(): pl.pallas_call(kernel, in_specs=[pl.BlockSpec(memory_space=pltpu.SMEM)] +...  7.56 us
  transfers between devices with their start and end apart: 12, of which 7 were waited for; matrix products, arithmetic and copies ran while one was open for 3% of the time, Pallas kernels for 7%

profile of v4, /device:TPU:2, one launch (start us, length us, event | category | flops | bytes accessed | tf_op | source)
XLA Modules:
  0.0 194.6 jit_solution(7077349451498363908)
XLA Ops:
  7.2 1.6 broadcast_in_dim.10
  8.8 16.7 %all-to-all-start = ((bf16[32,64,128]{2,1,0:T(8,128)(2,1)}), bf16[32,64,128]{2,1,0:T(8,128)(2,1)S(1)}, u32[]{:S(2)}, u32[]{:S(2)}) async-start(bf16[32,64,128]{2,1,0:T(8,128)(2,1)} %broadcast_in_dim.10), calls=%async_computation | async-start | bytes 1048576 | tf_op jit(solution)/shard_map/all_to_all | solution.py:19
  25.6 2.0 %shard_map.162 = (bf16[272,128]{1,0:T(8,128)(2,1)}, bf16[272,128]{1,0:T(8,128)(2,1)}) custom-call(f32[1,64]{1,0:T(1,128)} %bitcast.33, f32[64,172]{1,0:T(8,128)} %refs_1_.1, f32[64,172]{1,0:T(8,128)} %refs_2_.1, f32[64,172]{1,0:T(8,128)} %bitcast.30, f32[1,64]{1,0:T(1,128)} %bitcast.34, f32[64,172]{1,0:T(8,128)} %refs_5_.1, f32[64,172]{1,0:T(8,128)} %refs_6_.1, ...), custom_call_target="tpu_custom_call" | custom-call | tf_op jit(solution)/shard_map/pallas_call | solution.py:59
  27.6 36.1 %all_gather.6.refs_0_ = bf16[2176,128]{1,0:T(8,128)(2,1)S(1)} all-gather(bf16[272,128]{1,0:T(8,128)(2,1)} %get-tuple-element.17), channel_id=1, replica_groups=mesh['pair'=8,'parity'=2,'core'=2,'tp_0'=8,'tp_1'=4] {'pair'}, dimensions={0}, use_global_device_ids=true | all-gather | bytes 626688 | tf_op jit(solution)/shard_map/all_gather | solution.py:219
  63.7 6.0 %collective-permute-start.1 = (bf16[1360,128]{1,0:T(8,128)(2,1)S(1)}, bf16[1360,128]{1,0:T(8,128)(2,1)S(1)}, u32[]{:S(2)}, u32[]{:S(2)}) collective-permute-start(bf16[1360,128]{1,0:T(8,128)(2,1)S(1)} %slice.16), channel_id=1, source_target_pairs={{0,960},{64,0},{128,64},{192,128},{256,192},{320,256},{384,320},{4... | collective-permute-start | bytes 1044488 | tf_op jit(solution)/shard_map/ppermute | solution.py:74
  69.8 1.9 collective-permute-start
  71.7 1.9 collective-permute-start.2
  73.6 0.9 collective-permute-done.1.refs_2_
  74.5 1.9 collective-permute-start.3
  76.4 5.9 %collective-permute-done.2.refs_3_ = bf16[816,128]{1,0:T(8,128)(2,1)S(1)} collective-permute-done((bf16[816,128]{1,0:T(8,128)(2,1)S(1)}, bf16[816,128]{1,0:T(8,128)(2,1)S(1)}, u32[]{:S(2)}, u32[]{:S(2)}) %collective-permute-start.2) | collective-permute-done | bytes 208928 | tf_op jit(solution)/shard_map/ppermute | solution.py:75
  82.4 1.9 collective-permute-start.4
  84.9 0.8 collective-permute-done.4.refs_5_
  86.9 3.8 %shard_map.163 = bf16[2048,128]{1,0:T(8,128)(2,1)} custom-call(s32[2]{0:T(128)} %pad_add_fusion.place_ref, bf16[2176,128]{1,0:T(8,128)(2,1)} %copy-done, bf16[2176,128]{1,0:T(8,128)(2,1)} %copy-done.3, bf16[1360,128]{1,0:T(8,128)(2,1)} %copy-done.6, bf16[816,128]{1,0:T(8,128)(2,1)} %copy-done.8, bf16[1360,128]{1,0:T(8,128)(2,1)} %copy-done.7, ...), custom_call_target="tpu_custom_call" | custom-call | tf_op jit(solution)/shard_map/pallas_call | solution.py:157
  90.7 26.7 %all_to_all.25 = bf16[32,64,128]{2,1,0:T(8,128)(2,1)S(1)} all-to-all(bf16[32,64,128]{2,1,0:T(8,128)(2,1)} %bitcast.28), channel_id=1, replica_groups=mesh['pair'=8,'parity'=2,'core'=2,'tp_0'=8,'tp_1'=4] {'tp_0','tp_1'}, dimensions={0} | all-to-all | bytes 1048576 | tf_op jit(solution)/shard_map/all_to_all | solution.py:28
  117.4 0.9 broadcast_in_dim.13
  118.4 5.6 %all-to-all-start.2 = ((bf16[32,64,128]{2,1,0:T(8,128)(2,1)}), bf16[32,64,128]{2,1,0:T(8,128)(2,1)S(1)}, u32[]{:S(2)}, u32[]{:S(2)}) async-start(bf16[32,64,128]{2,1,0:T(8,128)(2,1)} %broadcast_in_dim.13), calls=%async_computation.2 | async-start | bytes 1048576 | tf_op jit(solution)/shard_map/all_to_all | solution.py:19
  124.0 1.3 fusion.4
  125.3 1.9 collective-permute-start.5
  127.3 3.9 %collective-permute-start.6 = (bf16[2176,128]{1,0:T(8,128)(2,1)S(1)}, bf16[2176,128]{1,0:T(8,128)(2,1)S(1)}, u32[]{:S(2)}, u32[]{:S(2)}) collective-permute-start(bf16[2176,128]{1,0:T(8,128)(2,1)S(1)} %get-tuple-element.27), channel_id=1, source_target_pairs={{0,64},{64,128},{128,192},{192,256},{256,320},{320,384},{384,448},... | collective-permute-start | bytes 1671176 | tf_op jit(solution)/shard_map/ppermute | solution.py:75
  131.2 8.7 %all-to-all-done.2 = bf16[32,64,128]{2,1,0:T(8,128)(2,1)S(1)} async-done(((bf16[32,64,128]{2,1,0:T(8,128)(2,1)}), bf16[32,64,128]{2,1,0:T(8,128)(2,1)S(1)}, u32[]{:S(2)}, u32[]{:S(2)}) %all-to-all-start.2) | async-done | bytes 524320 | tf_op jit(solution)/shard_map/all_to_all | solution.py:19
  140.2 1.1 fusion.2.refs_3_
  141.4 2.0 %collective-permute-done.6.refs_2_ = bf16[2176,128]{1,0:T(8,128)(2,1)S(1)} collective-permute-done((bf16[2176,128]{1,0:T(8,128)(2,1)S(1)}, bf16[2176,128]{1,0:T(8,128)(2,1)S(1)}, u32[]{:S(2)}, u32[]{:S(2)}) %collective-permute-start.6) | collective-permute-done | bytes 557088 | tf_op jit(solution)/shard_map/ppermute | solution.py:75
  143.3 0.8 copy-done.5
  144.1 3.8 %shard_map.164 = bf16[2048,128]{1,0:T(8,128)(2,1)} custom-call(s32[2]{0:T(128)} %pad_add_fusion.place_ref, bf16[4352,128]{1,0:T(8,128)(2,1)} %all-gather.2.cloned.1.call-done.refs_0_, bf16[2176,128]{1,0:T(8,128)(2,1)} %copy-done.4, bf16[2176,128]{1,0:T(8,128)(2,1)} %copy-done.5, bf16[2048,128]{1,0:T(8,128)(2,1)} %fusion.2.refs_3_), custom_call_target="tpu_custom_call" | custom-call | tf_op jit(solution)/shard_map/pallas_call | solution.py:157
  147.9 9.8 %all-to-all-start.3 = ((bf16[32,64,128]{2,1,0:T(8,128)(2,1)}), bf16[32,64,128]{2,1,0:T(8,128)(2,1)S(1)}, u32[]{:S(2)}, u32[]{:S(2)}) async-start(bf16[32,64,128]{2,1,0:T(8,128)(2,1)} %bitcast.27), calls=%async_computation.3 | async-start | bytes 1048576 | tf_op jit(solution)/shard_map/all_to_all | solution.py:28
  157.7 0.8 dynamic-slice_multiply_fusion
  158.5 3.7 %shard_map.165 = (bf16[172,2048]{1,0:T(8,128)(2,1)}, bf16[172,2048]{1,0:T(8,128)(2,1)}, bf16[172,2048]{1,0:T(8,128)(2,1)}) custom-call(s32[2]{0:T(128)} %pad_add_fusion.place_ref, bf16[2176,128]{1,0:T(8,128)(2,1)} %copy-done, bf16[2176,128]{1,0:T(8,128)(2,1)} %copy-done.3, bf16[1360,128]{1,0:T(8,128)(2,1)} %copy-done.6, bf16[816,128]{1,0:T(8,128)(2,1)} %copy-done.8, ...), custom_call_target="tpu_custom_call" | custom-call | tf_op jit(solution)/shard_map/pallas_call | solution.py:188
  162.2 3.6 %shard_map.166 = (bf16[172,2048]{1,0:T(8,128)(2,1)}, bf16[172,2048]{1,0:T(8,128)(2,1)}, bf16[172,2048]{1,0:T(8,128)(2,1)}) custom-call(s32[2]{0:T(128)} %pad_add_fusion.place_ref, bf16[4352,128]{1,0:T(8,128)(2,1)} %all-gather.2.cloned.1.call-done.refs_0_, bf16[2176,128]{1,0:T(8,128)(2,1)} %copy-done.4, bf16[2176,128]{1,0:T(8,128)(2,1)} %copy-done.5), custom_call_target="tpu_custom_call" | custom-call | tf_op jit(solution)/shard_map/pallas_call | solution.py:188
  165.7 6.5 %all-to-all-done.3 = bf16[32,64,128]{2,1,0:T(8,128)(2,1)S(1)} async-done(((bf16[32,64,128]{2,1,0:T(8,128)(2,1)}), bf16[32,64,128]{2,1,0:T(8,128)(2,1)S(1)}, u32[]{:S(2)}, u32[]{:S(2)}) %all-to-all-start.3) | async-done | bytes 524320 | tf_op jit(solution)/shard_map/all_to_all | solution.py:28
  173.0 5.6 %all-to-all-start.4 = ((f32[32,1,128]{2,1,0:T(1,128)}), f32[32,1,128]{2,1,0:T(1,128)S(1)}, u32[]{:S(2)}, u32[]{:S(2)}) async-start(f32[32,1,128]{2,1,0:T(1,128)} %broadcast_in_dim.14), calls=%async_computation.4 | async-start | bytes 32768 | tf_op jit(solution)/shard_map/all_to_all | solution.py:19
  178.6 0.7 dynamic-slice_convert_fusion
  179.3 7.7 %all-to-all-done.4 = f32[32,1,128]{2,1,0:T(1,128)S(1)} async-done(((f32[32,1,128]{2,1,0:T(1,128)}), f32[32,1,128]{2,1,0:T(1,128)S(1)}, u32[]{:S(2)}, u32[]{:S(2)}) %all-to-all-start.4) | async-done | bytes 16416 | tf_op jit(solution)/shard_map/all_to_all | solution.py:19
  (40 shorter events, 3.7 us)
Async XLA Ops:
  8.8 77.0 %all-to-all-start = ((bf16[32,64,128]{2,1,0:T(8,128)(2,1)}), bf16[32,64,128]{2,1,0:T(8,128)(2,1)S(1)}, u32[]{:S(2)}, u32[]{:S(2)}) async-start(bf16[32,64,128]{2,1,0:T(8,128)(2,1)} %broadcast_in_dim.10), calls=%async_computation | async-start | bytes 1048576 | tf_op jit(solution)/shard_map/all_to_all | solution.py:19
  25.5 98.5 %all-gather.2.cloned.1.call-start = ((), (), s32[]{:S(2)}) async-start(), calls=%async_computation.5 | async-start | bytes 1183744 | tf_op jit(solution)/shard_map/all_gather | solution.py:218
  63.7 22.1 %copy-start = (bf16[2176,128]{1,0:T(8,128)(2,1)}, bf16[2176,128]{1,0:T(8,128)(2,1)S(1)}, u32[]{:S(2)}) copy-start(bf16[2176,128]{1,0:T(8,128)(2,1)S(1)} %all_gather.6.refs_0_) | copy-start | bytes 1671172
  63.7 10.8 %collective-permute-start.1 = (bf16[1360,128]{1,0:T(8,128)(2,1)S(1)}, bf16[1360,128]{1,0:T(8,128)(2,1)S(1)}, u32[]{:S(2)}, u32[]{:S(2)}) collective-permute-start(bf16[1360,128]{1,0:T(8,128)(2,1)S(1)} %slice.16), channel_id=1, source_target_pairs={{0,960},{64,0},{128,64},{192,128},{256,192},{320,256},{384,320},{4... | collective-permute-start | bytes 1044488 | tf_op jit(solution)/shard_map/ppermute | solution.py:74
  69.8 16.0 %collective-permute-start = (bf16[2176,128]{1,0:T(8,128)(2,1)S(1)}, bf16[2176,128]{1,0:T(8,128)(2,1)S(1)}, u32[]{:S(2)}, u32[]{:S(2)}) collective-permute-start(bf16[2176,128]{1,0:T(8,128)(2,1)S(1)} %all_gather.6.refs_0_), channel_id=1, source_target_pairs={{0,32},{32,0},{1,33},{33,1},{2,34},{34,2},{3,35},{35,3},{4,36},{36... | collective-permute-start | bytes 1671176 | tf_op jit(solution)/shard_map/ppermute | solution.py:80
  71.7 10.7 %collective-permute-start.2 = (bf16[816,128]{1,0:T(8,128)(2,1)S(1)}, bf16[816,128]{1,0:T(8,128)(2,1)S(1)}, u32[]{:S(2)}, u32[]{:S(2)}) collective-permute-start(bf16[816,128]{1,0:T(8,128)(2,1)S(1)} %slice.17), channel_id=1, source_target_pairs={{0,64},{64,128},{128,192},{192,256},{256,320},{320,384},{384,448},... | collective-permute-start | bytes 626696 | tf_op jit(solution)/shard_map/ppermute | solution.py:75
  74.5 11.3 %copy-start.6 = (bf16[1360,128]{1,0:T(8,128)(2,1)}, bf16[1360,128]{1,0:T(8,128)(2,1)S(1)}, u32[]{:S(2)}) copy-start(bf16[1360,128]{1,0:T(8,128)(2,1)S(1)} %collective-permute-done.1.refs_2_) | copy-start | bytes 1044484
  74.5 11.2 %collective-permute-start.3 = (bf16[1360,128]{1,0:T(8,128)(2,1)S(1)}, bf16[1360,128]{1,0:T(8,128)(2,1)S(1)}, u32[]{:S(2)}, u32[]{:S(2)}) collective-permute-start(bf16[1360,128]{1,0:T(8,128)(2,1)S(1)} %collective-permute-done.1.refs_2_), channel_id=1, source_target_pairs={{0,32},{32,0},{1,33},{33,1},{2,34},{34,2},{3,35},{35,3},{4,36},{36... | collective-permute-start | bytes 1044488 | tf_op jit(solution)/shard_map/ppermute | solution.py:80
  82.4 3.4 %copy-start.8 = (bf16[816,128]{1,0:T(8,128)(2,1)}, bf16[816,128]{1,0:T(8,128)(2,1)S(1)}, u32[]{:S(2)}) copy-start(bf16[816,128]{1,0:T(8,128)(2,1)S(1)} %collective-permute-done.2.refs_3_) | copy-start | bytes 626692
  82.4 3.3 %collective-permute-start.4 = (bf16[816,128]{1,0:T(8,128)(2,1)S(1)}, bf16[816,128]{1,0:T(8,128)(2,1)S(1)}, u32[]{:S(2)}, u32[]{:S(2)}) collective-permute-start(bf16[816,128]{1,0:T(8,128)(2,1)S(1)} %collective-permute-done.2.refs_3_), channel_id=1, source_target_pairs={{0,32},{32,0},{1,33},{33,1},{2,34},{34,2},{3,35},{35,3},{4,36},{36... | collective-permute-start | bytes 626696 | tf_op jit(solution)/shard_map/ppermute | solution.py:80
  85.7 0.7 copy-start.9
  85.7 0.9 copy-start.3
  85.7 1.0 copy-start.7
  85.8 1.1 copy-start.1
  118.4 21.5 %all-to-all-start.2 = ((bf16[32,64,128]{2,1,0:T(8,128)(2,1)}), bf16[32,64,128]{2,1,0:T(8,128)(2,1)S(1)}, u32[]{:S(2)}, u32[]{:S(2)}) async-start(bf16[32,64,128]{2,1,0:T(8,128)(2,1)} %broadcast_in_dim.13), calls=%async_computation.2 | async-start | bytes 1048576 | tf_op jit(solution)/shard_map/all_to_all | solution.py:19
  123.9 16.3 %copy-start.2 = (bf16[32,64,128]{2,1,0:T(8,128)(2,1)S(1)}, bf16[32,64,128]{2,1,0:T(8,128)(2,1)}, u32[]{:S(2)}) copy-start(bf16[32,64,128]{2,1,0:T(8,128)(2,1)} %copy-done.1) | copy-start | bytes 1572868
  123.9 16.3 %copy-start.10 = (f32[2048]{0:T(1024)S(1)}, f32[2048]{0:T(1024)}, u32[]{:S(2)}) copy-start(f32[2048]{0:T(1024)} %param.16) | copy-start | bytes 24580
  125.3 16.0 %collective-permute-start.5 = (bf16[2176,128]{1,0:T(8,128)(2,1)S(1)}, bf16[2176,128]{1,0:T(8,128)(2,1)S(1)}, u32[]{:S(2)}, u32[]{:S(2)}) collective-permute-start(bf16[2176,128]{1,0:T(8,128)(2,1)S(1)} %get-tuple-element.28), channel_id=1, source_target_pairs={{0,960},{64,0},{128,64},{192,128},{256,192},{320,256},{384,320},{4... | collective-permute-start | bytes 1671176 | tf_op jit(solution)/shard_map/ppermute | solution.py:74
  127.3 16.1 %collective-permute-start.6 = (bf16[2176,128]{1,0:T(8,128)(2,1)S(1)}, bf16[2176,128]{1,0:T(8,128)(2,1)S(1)}, u32[]{:S(2)}, u32[]{:S(2)}) collective-permute-start(bf16[2176,128]{1,0:T(8,128)(2,1)S(1)} %get-tuple-element.27), channel_id=1, source_target_pairs={{0,64},{64,128},{128,192},{192,256},{256,320},{320,384},{384,448},... | collective-permute-start | bytes 1671176 | tf_op jit(solution)/shard_map/ppermute | solution.py:75
  141.4 2.0 %copy-start.4 = (bf16[2176,128]{1,0:T(8,128)(2,1)}, bf16[2176,128]{1,0:T(8,128)(2,1)S(1)}, u32[]{:S(2)}) copy-start(bf16[2176,128]{1,0:T(8,128)(2,1)S(1)} %collective-permute-done.5.refs_1_) | copy-start | bytes 1671172
  143.3 0.8 copy-start.5
  147.9 24.3 %all-to-all-start.3 = ((bf16[32,64,128]{2,1,0:T(8,128)(2,1)}), bf16[32,64,128]{2,1,0:T(8,128)(2,1)S(1)}, u32[]{:S(2)}, u32[]{:S(2)}) async-start(bf16[32,64,128]{2,1,0:T(8,128)(2,1)} %bitcast.27), calls=%async_computation.3 | async-start | bytes 1048576 | tf_op jit(solution)/shard_map/all_to_all | solution.py:28
  173.0 14.1 %all-to-all-start.4 = ((f32[32,1,128]{2,1,0:T(1,128)}), f32[32,1,128]{2,1,0:T(1,128)S(1)}, u32[]{:S(2)}, u32[]{:S(2)}) async-start(f32[32,1,128]{2,1,0:T(1,128)} %broadcast_in_dim.14), calls=%async_computation.4 | async-start | bytes 32768 | tf_op jit(solution)/shard_map/all_to_all | solution.py:19
Sparse Core Ops, SparseCore 0:
  69.9 48.3 all-gather.1

commit v5 on v4

--- a/solution.py
+++ b/solution.py
@@ -40,13 +40,15 @@
     return aligned(-(-3 * aligned(hidden) // 2))
 
 
-def packed(*groups):
+def packed(peers, tokens, *groups):
     rows, hidden = groups[0][1].shape
     block, half = aligned(hidden), packed_rows(hidden)
     count = len(groups)
 
     def kernel(*refs):
-        outs, tall_ref = refs[4 * count : -1], refs[-1]
+        tokens_ref, copies_ref, tall_ref = refs[4 * count], refs[-2], refs[-1]
+        outs = refs[4 * count + 1 : -2]
+        copies_ref[...] = jnp.broadcast_to(tokens_ref[...][None], copies_ref.shape)
         tall_ref[...] = jnp.zeros_like(tall_ref)
         for i, out_ref in enumerate(outs):
             gain_ref, gate_ref, up_ref, down_ref = refs[4 * i : 4 * i + 4]
@@ -58,9 +60,10 @@
 
     return pl.pallas_call(
         kernel,
-        out_shape=[jax.ShapeDtypeStruct((half, 2 * rows), jnp.bfloat16)] * count,
+        out_shape=[jax.ShapeDtypeStruct((half, 2 * rows), jnp.bfloat16)] * count
+        + [jax.ShapeDtypeStruct((peers, *tokens.shape), tokens.dtype)],
         scratch_shapes=[pltpu.VMEM((count, 2 * half, rows), jnp.float32)],
-    )(*(a for gain, gate, up, down in groups for a in (gain[None, :], gate, up, down.T)))
+    )(*(a for gain, gate, up, down in groups for a in (gain[None, :], gate, up, down.T)), tokens)
 
 
 def first_share(pairs, alone):
@@ -209,12 +212,14 @@
     columns = tokens.shape[1]
     hidden = first_gate.shape[1]
     column_start = lax.axis_index(TP) * columns
-    full = gathered_copies(tokens.T, TP)
     place = jnp.stack([lax.axis_index("parity"), lax.axis_index("core")]).astype(jnp.int32)
-    rows_one, rows_two = packed(
+    rows_one, rows_two, copies = packed(
+        lax.axis_size(TP),
+        tokens.T,
         (first_gain, first_gate, first_up, first_down),
         (second_gain, second_gate, second_up, second_down),
     )
+    full = lax.all_to_all(copies, TP, 0, 0, tiled=True).reshape(-1, tokens.shape[0])
     own_two = lax.all_gather(rows_two, ("pair", "core"), axis=0, tiled=True)
     own_one = lax.all_gather(rows_one, "pair", axis=0, tiled=True)
     near_one = from_neighbours(own_one, True)

time: 196 us -> 194 us (0.990)
    all_to_all x0 -> x1, starting transfers between devices: none -> 16.7 us  [on_device(): lax.all_to_all(copies, TP, 0, 0, tiled=True).reshape(-1, tokens.shape[0])]
    all_to_all x3 -> x2, starting transfers between devices: 27.8 us -> 11.1 us  [sent_to_all(): lax.all_to_all(jnp.broadcast_to(x[None], (peers, *x.shape)), axis, 0, 0,...]
    all_to_all x3 -> x2, waiting for transfers between devices: 16.5 us -> 16.5 us  [sent_to_all(): lax.all_to_all(jnp.broadcast_to(x[None], (peers, *x.shape)), axis, 0, 0,...]
  transfers between devices with their start and end apart: 12 -> 12, of which waited for: 7 -> 7; matrix products, arithmetic and copies ran while one was open for 3% -> 3% of each run, Pallas kernels for 7% -> 6%
where the time goes in v5:
time: 194 us; the launch traced here: 193 us
  blocking collectives  63.2 us (33%)
  starting transfers between devices  56.8 us (29%)
  waiting for transfers between devices  32.6 us (17%)
  Pallas kernels  17 us (9%)
  between operations  14.3 us (7%)
  local copies, waits for them, and re-layouts  4.83 us (2%)
  other arithmetic  4.47 us (2%)
    all_gather x1, blocking collectives, on_device(): own_one = lax.all_gather(rows_one, 'pair', axis=0, tiled=True)  36.2 us
    all_to_all x1, blocking collectives, sent_and_summed(): lax.all_to_all(x.reshape(peers, -1, *x.shape[1:]), axis, 0, 0, tiled=True)  27 us
    all_to_all x1, starting transfers between devices, on_device(): lax.all_to_all(copies, TP, 0, 0, tiled=True).reshape(-1, tokens.shape[0])  16.7 us
    all_to_all x2, waiting for transfers between devices, sent_to_all(): lax.all_to_all(jnp.broadcast_to(x[None], (peers, *x.shape)), axis, 0, 0,...  16.5 us
    all_to_all x2, starting transfers between devices, sent_to_all(): lax.all_to_all(jnp.broadcast_to(x[None], (peers, *x.shape)), axis, 0, 0,...  11.1 us
    all_to_all x1, starting transfers between devices, sent_and_summed(): lax.all_to_all(x.reshape(peers, -1, *x.shape[1:]), axis, 0, 0, tiled=True)  9.78 us
    ppermute x2, waiting for transfers between devices, from_neighbours(): lax.ppermute(own[cut:], FS[:2], [(i, (i + 1) % ring) for i in range(ring)])  7.89 us
    ppermute x2, starting transfers between devices, from_neighbours(): lax.ppermute(own[:cut], FS[:2], [(i, (i - 1) % ring) for i in range(ring)])  7.6 us
  transfers between devices with their start and end apart: 12, of which 7 were waited for; matrix products, arithmetic and copies ran while one was open for 3% of the time, Pallas kernels for 6%

profile of v5, /device:TPU:2, one launch (start us, length us, event | category | flops | bytes accessed | tf_op | source)
XLA Modules:
  0.0 193.2 jit_solution(13557095109110999476)
XLA Ops:
  7.2 2.2 %shard_map.162 = (bf16[272,128]{1,0:T(8,128)(2,1)}, bf16[272,128]{1,0:T(8,128)(2,1)}, bf16[32,64,128]{2,1,0:T(8,128)(2,1)}) custom-call(f32[1,64]{1,0:T(1,128)} %bitcast.33, f32[64,172]{1,0:T(8,128)} %refs_1_.1, f32[64,172]{1,0:T(8,128)} %refs_2_.1, f32[64,172]{1,0:T(8,128)} %bitcast.29, f32[1,64]{1,0:T(1,128)} %bitcast.34, f32[64,172]{1,0:T(8,128)} %refs_5_.1, ...), custom_call_target="tpu_custom_call" | custom-call | tf_op jit(solution)/shard_map/pallas_call | solution.py:61
  9.4 16.7 %all-to-all-start = ((bf16[32,64,128]{2,1,0:T(8,128)(2,1)}), bf16[32,64,128]{2,1,0:T(8,128)(2,1)S(1)}, u32[]{:S(2)}, u32[]{:S(2)}) async-start(bf16[32,64,128]{2,1,0:T(8,128)(2,1)} %get-tuple-element.18), calls=%async_computation | async-start | bytes 1048576 | tf_op jit(solution)/shard_map/all_to_all | solution.py:222
  26.1 36.2 %all_gather.6.refs_0_ = bf16[2176,128]{1,0:T(8,128)(2,1)S(1)} all-gather(bf16[272,128]{1,0:T(8,128)(2,1)} %get-tuple-element.19), channel_id=1, replica_groups=mesh['pair'=8,'parity'=2,'core'=2,'tp_0'=8,'tp_1'=4] {'pair'}, dimensions={0}, use_global_device_ids=true | all-gather | bytes 626688 | tf_op jit(solution)/shard_map/all_gather | solution.py:224
  62.4 5.7 %collective-permute-start.1 = (bf16[1360,128]{1,0:T(8,128)(2,1)S(1)}, bf16[1360,128]{1,0:T(8,128)(2,1)S(1)}, u32[]{:S(2)}, u32[]{:S(2)}) collective-permute-start(bf16[1360,128]{1,0:T(8,128)(2,1)S(1)} %slice.16), channel_id=1, source_target_pairs={{0,960},{64,0},{128,64},{192,128},{256,192},{320,256},{384,320},{4... | collective-permute-start | bytes 1044488 | tf_op jit(solution)/shard_map/ppermute | solution.py:77
  68.1 1.9 collective-permute-start
  70.1 1.9 collective-permute-start.2
  72.0 0.9 collective-permute-done.1.refs_2_
  72.9 1.9 collective-permute-start.3
  74.8 5.9 %collective-permute-done.2.refs_3_ = bf16[816,128]{1,0:T(8,128)(2,1)S(1)} collective-permute-done((bf16[816,128]{1,0:T(8,128)(2,1)S(1)}, bf16[816,128]{1,0:T(8,128)(2,1)S(1)}, u32[]{:S(2)}, u32[]{:S(2)}) %collective-permute-start.2) | collective-permute-done | bytes 208928 | tf_op jit(solution)/shard_map/ppermute | solution.py:78
  80.7 1.9 collective-permute-start.4
  82.7 0.6 pad_add_fusion.place_ref
  83.3 0.8 collective-permute-done.4.refs_5_
  85.2 3.8 %shard_map.163 = bf16[2048,128]{1,0:T(8,128)(2,1)} custom-call(s32[2]{0:T(128)} %pad_add_fusion.place_ref, bf16[2176,128]{1,0:T(8,128)(2,1)} %copy-done, bf16[2176,128]{1,0:T(8,128)(2,1)} %copy-done.3, bf16[1360,128]{1,0:T(8,128)(2,1)} %copy-done.6, bf16[816,128]{1,0:T(8,128)(2,1)} %copy-done.8, bf16[1360,128]{1,0:T(8,128)(2,1)} %copy-done.7, ...), custom_call_target="tpu_custom_call" | custom-call | tf_op jit(solution)/shard_map/pallas_call | solution.py:160
  89.0 27.0 %all_to_all.25 = bf16[32,64,128]{2,1,0:T(8,128)(2,1)S(1)} all-to-all(bf16[32,64,128]{2,1,0:T(8,128)(2,1)} %bitcast.28), channel_id=1, replica_groups=mesh['pair'=8,'parity'=2,'core'=2,'tp_0'=8,'tp_1'=4] {'tp_0','tp_1'}, dimensions={0} | all-to-all | bytes 1048576 | tf_op jit(solution)/shard_map/all_to_all | solution.py:28
  116.1 0.9 broadcast_in_dim.10
  117.0 5.6 %all-to-all-start.2 = ((bf16[32,64,128]{2,1,0:T(8,128)(2,1)}), bf16[32,64,128]{2,1,0:T(8,128)(2,1)S(1)}, u32[]{:S(2)}, u32[]{:S(2)}) async-start(bf16[32,64,128]{2,1,0:T(8,128)(2,1)} %broadcast_in_dim.10), calls=%async_computation.2 | async-start | bytes 1048576 | tf_op jit(solution)/shard_map/all_to_all | solution.py:19
  122.6 1.3 fusion.4
  124.0 1.9 collective-permute-start.5
  125.9 3.9 %collective-permute-start.6 = (bf16[2176,128]{1,0:T(8,128)(2,1)S(1)}, bf16[2176,128]{1,0:T(8,128)(2,1)S(1)}, u32[]{:S(2)}, u32[]{:S(2)}) collective-permute-start(bf16[2176,128]{1,0:T(8,128)(2,1)S(1)} %get-tuple-element.29), channel_id=1, source_target_pairs={{0,64},{64,128},{128,192},{192,256},{256,320},{320,384},{384,448},... | collective-permute-start | bytes 1671176 | tf_op jit(solution)/shard_map/ppermute | solution.py:78
  129.8 8.7 %all-to-all-done.2 = bf16[32,64,128]{2,1,0:T(8,128)(2,1)S(1)} async-done(((bf16[32,64,128]{2,1,0:T(8,128)(2,1)}), bf16[32,64,128]{2,1,0:T(8,128)(2,1)S(1)}, u32[]{:S(2)}, u32[]{:S(2)}) %all-to-all-start.2) | async-done | bytes 524320 | tf_op jit(solution)/shard_map/all_to_all | solution.py:19
  138.9 1.1 fusion.2.refs_3_
  140.0 2.0 %collective-permute-done.6.refs_2_ = bf16[2176,128]{1,0:T(8,128)(2,1)S(1)} collective-permute-done((bf16[2176,128]{1,0:T(8,128)(2,1)S(1)}, bf16[2176,128]{1,0:T(8,128)(2,1)S(1)}, u32[]{:S(2)}, u32[]{:S(2)}) %collective-permute-start.6) | collective-permute-done | bytes 557088 | tf_op jit(solution)/shard_map/ppermute | solution.py:78
  142.0 0.8 copy-done.5
  142.8 3.8 %shard_map.164 = bf16[2048,128]{1,0:T(8,128)(2,1)} custom-call(s32[2]{0:T(128)} %pad_add_fusion.place_ref, bf16[4352,128]{1,0:T(8,128)(2,1)} %all-gather.2.cloned.1.call-done.refs_0_, bf16[2176,128]{1,0:T(8,128)(2,1)} %copy-done.4, bf16[2176,128]{1,0:T(8,128)(2,1)} %copy-done.5, bf16[2048,128]{1,0:T(8,128)(2,1)} %fusion.2.refs_3_), custom_call_target="tpu_custom_call" | custom-call | tf_op jit(solution)/shard_map/pallas_call | solution.py:160
  146.5 9.8 %all-to-all-start.3 = ((bf16[32,64,128]{2,1,0:T(8,128)(2,1)}), bf16[32,64,128]{2,1,0:T(8,128)(2,1)S(1)}, u32[]{:S(2)}, u32[]{:S(2)}) async-start(bf16[32,64,128]{2,1,0:T(8,128)(2,1)} %bitcast.27), calls=%async_computation.3 | async-start | bytes 1048576 | tf_op jit(solution)/shard_map/all_to_all | solution.py:28
  156.3 0.8 dynamic-slice_multiply_fusion
  157.1 3.7 %shard_map.165 = (bf16[172,2048]{1,0:T(8,128)(2,1)}, bf16[172,2048]{1,0:T(8,128)(2,1)}, bf16[172,2048]{1,0:T(8,128)(2,1)}) custom-call(s32[2]{0:T(128)} %pad_add_fusion.place_ref, bf16[2176,128]{1,0:T(8,128)(2,1)} %copy-done, bf16[2176,128]{1,0:T(8,128)(2,1)} %copy-done.3, bf16[1360,128]{1,0:T(8,128)(2,1)} %copy-done.6, bf16[816,128]{1,0:T(8,128)(2,1)} %copy-done.8, ...), custom_call_target="tpu_custom_call" | custom-call | tf_op jit(solution)/shard_map/pallas_call | solution.py:191
  160.8 3.6 %shard_map.166 = (bf16[172,2048]{1,0:T(8,128)(2,1)}, bf16[172,2048]{1,0:T(8,128)(2,1)}, bf16[172,2048]{1,0:T(8,128)(2,1)}) custom-call(s32[2]{0:T(128)} %pad_add_fusion.place_ref, bf16[4352,128]{1,0:T(8,128)(2,1)} %all-gather.2.cloned.1.call-done.refs_0_, bf16[2176,128]{1,0:T(8,128)(2,1)} %copy-done.4, bf16[2176,128]{1,0:T(8,128)(2,1)} %copy-done.5), custom_call_target="tpu_custom_call" | custom-call | tf_op jit(solution)/shard_map/pallas_call | solution.py:191
  164.4 6.5 %all-to-all-done.3 = bf16[32,64,128]{2,1,0:T(8,128)(2,1)S(1)} async-done(((bf16[32,64,128]{2,1,0:T(8,128)(2,1)}), bf16[32,64,128]{2,1,0:T(8,128)(2,1)S(1)}, u32[]{:S(2)}, u32[]{:S(2)}) %all-to-all-start.3) | async-done | bytes 524320 | tf_op jit(solution)/shard_map/all_to_all | solution.py:28
  171.7 5.6 %all-to-all-start.4 = ((f32[32,1,128]{2,1,0:T(1,128)}), f32[32,1,128]{2,1,0:T(1,128)S(1)}, u32[]{:S(2)}, u32[]{:S(2)}) async-start(f32[32,1,128]{2,1,0:T(1,128)} %broadcast_in_dim.11), calls=%async_computation.4 | async-start | bytes 32768 | tf_op jit(solution)/shard_map/all_to_all | solution.py:19
  177.2 0.7 dynamic-slice_convert_fusion
  178.0 7.7 %all-to-all-done.4 = f32[32,1,128]{2,1,0:T(1,128)S(1)} async-done(((f32[32,1,128]{2,1,0:T(1,128)}), f32[32,1,128]{2,1,0:T(1,128)S(1)}, u32[]{:S(2)}, u32[]{:S(2)}) %all-to-all-start.4) | async-done | bytes 16416 | tf_op jit(solution)/shard_map/all_to_all | solution.py:19
  (39 shorter events, 3.1 us)
Async XLA Ops:
  9.4 74.7 %all-to-all-start = ((bf16[32,64,128]{2,1,0:T(8,128)(2,1)}), bf16[32,64,128]{2,1,0:T(8,128)(2,1)S(1)}, u32[]{:S(2)}, u32[]{:S(2)}) async-start(bf16[32,64,128]{2,1,0:T(8,128)(2,1)} %get-tuple-element.18), calls=%async_computation | async-start | bytes 1048576 | tf_op jit(solution)/shard_map/all_to_all | solution.py:222
  26.1 96.5 %all-gather.2.cloned.1.call-start = ((), (), s32[]{:S(2)}) async-start(), calls=%async_computation.5 | async-start | bytes 1183744 | tf_op jit(solution)/shard_map/all_gather | solution.py:223
  62.4 21.8 %copy-start = (bf16[2176,128]{1,0:T(8,128)(2,1)}, bf16[2176,128]{1,0:T(8,128)(2,1)S(1)}, u32[]{:S(2)}) copy-start(bf16[2176,128]{1,0:T(8,128)(2,1)S(1)} %all_gather.6.refs_0_) | copy-start | bytes 1671172
  62.4 10.5 %collective-permute-start.1 = (bf16[1360,128]{1,0:T(8,128)(2,1)S(1)}, bf16[1360,128]{1,0:T(8,128)(2,1)S(1)}, u32[]{:S(2)}, u32[]{:S(2)}) collective-permute-start(bf16[1360,128]{1,0:T(8,128)(2,1)S(1)} %slice.16), channel_id=1, source_target_pairs={{0,960},{64,0},{128,64},{192,128},{256,192},{320,256},{384,320},{4... | collective-permute-start | bytes 1044488 | tf_op jit(solution)/shard_map/ppermute | solution.py:77
  68.1 16.0 %collective-permute-start = (bf16[2176,128]{1,0:T(8,128)(2,1)S(1)}, bf16[2176,128]{1,0:T(8,128)(2,1)S(1)}, u32[]{:S(2)}, u32[]{:S(2)}) collective-permute-start(bf16[2176,128]{1,0:T(8,128)(2,1)S(1)} %all_gather.6.refs_0_), channel_id=1, source_target_pairs={{0,32},{32,0},{1,33},{33,1},{2,34},{34,2},{3,35},{35,3},{4,36},{36... | collective-permute-start | bytes 1671176 | tf_op jit(solution)/shard_map/ppermute | solution.py:83
  70.1 10.7 %collective-permute-start.2 = (bf16[816,128]{1,0:T(8,128)(2,1)S(1)}, bf16[816,128]{1,0:T(8,128)(2,1)S(1)}, u32[]{:S(2)}, u32[]{:S(2)}) collective-permute-start(bf16[816,128]{1,0:T(8,128)(2,1)S(1)} %slice.17), channel_id=1, source_target_pairs={{0,64},{64,128},{128,192},{192,256},{256,320},{320,384},{384,448},... | collective-permute-start | bytes 626696 | tf_op jit(solution)/shard_map/ppermute | solution.py:78
  72.9 11.3 %copy-start.6 = (bf16[1360,128]{1,0:T(8,128)(2,1)}, bf16[1360,128]{1,0:T(8,128)(2,1)S(1)}, u32[]{:S(2)}) copy-start(bf16[1360,128]{1,0:T(8,128)(2,1)S(1)} %collective-permute-done.1.refs_2_) | copy-start | bytes 1044484
  72.9 11.2 %collective-permute-start.3 = (bf16[1360,128]{1,0:T(8,128)(2,1)S(1)}, bf16[1360,128]{1,0:T(8,128)(2,1)S(1)}, u32[]{:S(2)}, u32[]{:S(2)}) collective-permute-start(bf16[1360,128]{1,0:T(8,128)(2,1)S(1)} %collective-permute-done.1.refs_2_), channel_id=1, source_target_pairs={{0,32},{32,0},{1,33},{33,1},{2,34},{34,2},{3,35},{35,3},{4,36},{36... | collective-permute-start | bytes 1044488 | tf_op jit(solution)/shard_map/ppermute | solution.py:83
  80.7 3.4 %copy-start.8 = (bf16[816,128]{1,0:T(8,128)(2,1)}, bf16[816,128]{1,0:T(8,128)(2,1)S(1)}, u32[]{:S(2)}) copy-start(bf16[816,128]{1,0:T(8,128)(2,1)S(1)} %collective-permute-done.2.refs_3_) | copy-start | bytes 626692
  80.7 3.3 %collective-permute-start.4 = (bf16[816,128]{1,0:T(8,128)(2,1)S(1)}, bf16[816,128]{1,0:T(8,128)(2,1)S(1)}, u32[]{:S(2)}, u32[]{:S(2)}) collective-permute-start(bf16[816,128]{1,0:T(8,128)(2,1)S(1)} %collective-permute-done.2.refs_3_), channel_id=1, source_target_pairs={{0,32},{32,0},{1,33},{33,1},{2,34},{34,2},{3,35},{35,3},{4,36},{36... | collective-permute-start | bytes 626696 | tf_op jit(solution)/shard_map/ppermute | solution.py:83
  84.1 0.7 copy-start.9
  84.1 0.9 copy-start.3
  84.1 1.0 copy-start.7
  84.1 1.1 copy-start.1
  117.0 21.6 %all-to-all-start.2 = ((bf16[32,64,128]{2,1,0:T(8,128)(2,1)}), bf16[32,64,128]{2,1,0:T(8,128)(2,1)S(1)}, u32[]{:S(2)}, u32[]{:S(2)}) async-start(bf16[32,64,128]{2,1,0:T(8,128)(2,1)} %broadcast_in_dim.10), calls=%async_computation.2 | async-start | bytes 1048576 | tf_op jit(solution)/shard_map/all_to_all | solution.py:19
  122.6 16.3 %copy-start.2 = (bf16[32,64,128]{2,1,0:T(8,128)(2,1)S(1)}, bf16[32,64,128]{2,1,0:T(8,128)(2,1)}, u32[]{:S(2)}) copy-start(bf16[32,64,128]{2,1,0:T(8,128)(2,1)} %copy-done.1) | copy-start | bytes 1572868
  122.6 16.3 %copy-start.10 = (f32[2048]{0:T(1024)S(1)}, f32[2048]{0:T(1024)}, u32[]{:S(2)}) copy-start(f32[2048]{0:T(1024)} %param.16) | copy-start | bytes 24580
  124.0 16.0 %collective-permute-start.5 = (bf16[2176,128]{1,0:T(8,128)(2,1)S(1)}, bf16[2176,128]{1,0:T(8,128)(2,1)S(1)}, u32[]{:S(2)}, u32[]{:S(2)}) collective-permute-start(bf16[2176,128]{1,0:T(8,128)(2,1)S(1)} %get-tuple-element.30), channel_id=1, source_target_pairs={{0,960},{64,0},{128,64},{192,128},{256,192},{320,256},{384,320},{4... | collective-permute-start | bytes 1671176 | tf_op jit(solution)/shard_map/ppermute | solution.py:77
  125.9 16.1 %collective-permute-start.6 = (bf16[2176,128]{1,0:T(8,128)(2,1)S(1)}, bf16[2176,128]{1,0:T(8,128)(2,1)S(1)}, u32[]{:S(2)}, u32[]{:S(2)}) collective-permute-start(bf16[2176,128]{1,0:T(8,128)(2,1)S(1)} %get-tuple-element.29), channel_id=1, source_target_pairs={{0,64},{64,128},{128,192},{192,256},{256,320},{320,384},{384,448},... | collective-permute-start | bytes 1671176 | tf_op jit(solution)/shard_map/ppermute | solution.py:78
  140.0 2.0 %copy-start.4 = (bf16[2176,128]{1,0:T(8,128)(2,1)}, bf16[2176,128]{1,0:T(8,128)(2,1)S(1)}, u32[]{:S(2)}) copy-start(bf16[2176,128]{1,0:T(8,128)(2,1)S(1)} %collective-permute-done.5.refs_1_) | copy-start | bytes 1671172
  142.0 0.8 copy-start.5
  146.5 24.3 %all-to-all-start.3 = ((bf16[32,64,128]{2,1,0:T(8,128)(2,1)}), bf16[32,64,128]{2,1,0:T(8,128)(2,1)S(1)}, u32[]{:S(2)}, u32[]{:S(2)}) async-start(bf16[32,64,128]{2,1,0:T(8,128)(2,1)} %bitcast.27), calls=%async_computation.3 | async-start | bytes 1048576 | tf_op jit(solution)/shard_map/all_to_all | solution.py:28
  171.7 14.1 %all-to-all-start.4 = ((f32[32,1,128]{2,1,0:T(1,128)}), f32[32,1,128]{2,1,0:T(1,128)S(1)}, u32[]{:S(2)}, u32[]{:S(2)}) async-start(f32[32,1,128]{2,1,0:T(1,128)} %broadcast_in_dim.11), calls=%async_computation.4 | async-start | bytes 32768 | tf_op jit(solution)/shard_map/all_to_all | solution.py:19
Sparse Core Ops, SparseCore 0:
  68.2 48.3 all-gather.1
